TPU v7x, 256 devices: a whole 4x4x8 slice. The times are simulated.
256 devices in a mesh: sp: 16 (over y, x), tp: 16 (over z, core).
Axes of the slice: x: 4, y: 4, z: 8, core: 2. Of those that a mesh axis runs over, the one named last changes fastest.
Arguments:
- resid: bfloat16 [8192, 2048], P(('sp', 'tp')), may hold values from -6 to 6
- query_a: bfloat16 [8192, 16, 128], P('sp', 'tp'), may hold values from -16 to 16
- key_a: bfloat16 [8192, 16, 128], P('sp', 'tp'), may hold values from -16 to 16
- value_a: bfloat16 [8192, 16, 128], P('sp', 'tp'), may hold values from -6 to 6
- query_b: bfloat16 [8192, 16, 64], P('sp', 'tp'), may hold values from -16 to 16
- key_b: bfloat16 [8192, 16, 64], P('sp', 'tp'), may hold values from -16 to 16
- value_b: bfloat16 [8192, 16, 64], P('sp', 'tp'), may hold values from -6 to 6
- mix_a: float32 [16], P('tp'), may hold values from 0.3 to 0.8
- mix_b: float32 [16], P('tp'), may hold values from 0.3 to 0.8
- head_gain_a: float32 [128], replicated, may hold values from 0.1 to 1.9
- head_gain_b: float32 [64], replicated, may hold values from 0.1 to 1.9
- proj_a: bfloat16 [2048, 2048], P('tp'), may hold values from -0.109375 to 0.109375
- proj_b: bfloat16 [1024, 2048], P('tp'), may hold values from -0.109375 to 0.109375
- norm_gain: float32 [2048], replicated, may hold values from 0.1 to 1.9
- route_ids: int32 [8192, 2], P(('sp', 'tp')), may hold values from 0 to 15, all different within a row; in each aligned block of 32 rows (0 to 31, 32 to 63, ...) at most 6 rows name the same one
- route_weights: float32 [8192, 2], P(('sp', 'tp')), may hold values from 0.2 to 1
- expert_gate: bfloat16 [16, 2048, 6144], P('sp', None, 'tp'), may hold values from -0.125 to 0.125
- expert_up: bfloat16 [16, 2048, 6144], P('sp', None, 'tp'), may hold values from -0.125 to 0.125
- expert_down: bfloat16 [16, 6144, 2048], P('sp', 'tp'), may hold values from -0.078125 to 0.078125
Outputs:
- out: bfloat16 [8192, 2048], P(('sp', 'tp'))
Inputs may be any that keep to these rules, and one draw needn't show every extreme that they name: `route_ids`: each row names 2 different experts. Within the rows of one device (aligned blocks of 32 rows) no expert is named by more than 6 rows, and in every draw some device's block names some expert exactly 6 times.
All inputs are finite; a program needn't handle non-finite values.
Results may differ from a plain program's by a relative error of at most 0.02.
Values may be sent and summed in bfloat16 or wider, within the bound.
A program may use at most 128 MiB of HBM per device.

v0:
```python
import math

import jax
import jax.numpy as jnp
from jax import lax
from jax.sharding import PartitionSpec as P

EPS = 1e-06
NEG = -1e30
HEAD_SCALE = 1.0 - (0.8 - 0.6 * math.exp(-0.3))
KEY_STEP = 512


def sent_together(arrays, axis, dim, along):
    both = jnp.concatenate(arrays, axis=along)
    result, at, finished = (lax.all_gather(both, axis, axis=dim, tiled=True), 0, [])
    for a in arrays:
        finished.append(lax.slice_in_dim(result, at, at + a.shape[along], axis=along))
        at += a.shape[along]
    return tuple(finished)


def cut_along(value, dim, size):
    before, after = (value.shape[:dim], value.shape[dim + 1 :])
    return jnp.moveaxis(value.reshape(*before, size, -1, *after), dim, 0)


def sent_and_summed(value, axis, dim):
    parts = cut_along(value, dim, lax.axis_size(axis))
    arrived = lax.all_to_all(parts, axis, split_axis=0, concat_axis=0, tiled=True)
    return arrived.astype(jnp.float32).sum(axis=0)


def rms_scaled(values, gain):
    return values * lax.rsqrt(jnp.mean(values * values, axis=-1, keepdims=True) + EPS) * gain


def slot_numbers(route_rows, experts, capacity):
    count, top_count = route_rows.shape
    flat = route_rows.reshape(count * top_count)
    onehot = (flat[:, None] == jnp.arange(experts, dtype=jnp.int32)[None, :]).astype(jnp.int32)
    ranks = jnp.sum((jnp.cumsum(onehot, axis=0) - onehot) * onehot, axis=1)
    return (flat * capacity + ranks).reshape(count, top_count)


def empty_map(count, heads, width):
    return (
        jnp.zeros((count, heads, width), jnp.float32),
        jnp.full((heads, count), NEG, jnp.float32),
        jnp.zeros((heads, count), jnp.float32),
    )


def empty_group(query, value):
    return (
        empty_map(query.shape[0], query.shape[1], value.shape[2]),
        empty_map(query.shape[0], query.shape[1], value.shape[2]),
    )


def map_update(state, query, keys, values, allowed, scale):
    weighted, maximum, sums = state
    scores = jnp.einsum("qhd,khd->hqk", query, keys, preferred_element_type=jnp.float32) * scale
    scores = jnp.where(allowed[None], scores, NEG)
    fresh = jnp.maximum(maximum, jnp.max(scores, axis=2))
    weights = jnp.where(allowed[None], jnp.exp(scores - fresh[:, :, None]), 0.0)
    factor = jnp.exp(maximum - fresh)
    sums = sums * factor + jnp.sum(weights, axis=2)
    added = jnp.einsum(
        "hqk,khv->qhv", weights.astype(jnp.bfloat16), values, preferred_element_type=jnp.float32
    )
    weighted = weighted * jnp.transpose(factor)[:, :, None] + added
    return (weighted, fresh, sums)


def group_update(states, query, keys, values, allowed):
    width = query.shape[2] // 2
    scale = 1.0 / math.sqrt(width)
    return tuple(
        (
            map_update(
                states[which],
                query[:, :, which * width : (which + 1) * width],
                keys[:, :, which * width : (which + 1) * width],
                values,
                allowed,
                scale,
            )
            for which in range(2)
        )
    )


def set_update(carry, queries, pieces):
    rows_a, rows_b, query_pos = queries
    piece_key_a, piece_value_a, piece_key_b, piece_value_b = pieces
    length = piece_key_a.shape[0]
    step = math.gcd(length, KEY_STEP)
    latest = query_pos[-1]

    def inner(index, states):
        first = index * step

        def compute(current):
            keys_a = lax.dynamic_slice_in_dim(piece_key_a, first, step, 0)
            values_a = lax.dynamic_slice_in_dim(piece_value_a, first, step, 0)
            keys_b = lax.dynamic_slice_in_dim(piece_key_b, first, step, 0)
            values_b = lax.dynamic_slice_in_dim(piece_value_b, first, step, 0)
            key_pos = first + jnp.arange(step, dtype=jnp.int32)
            allowed = key_pos[None, :] <= query_pos[:, None]
            return (
                group_update(current[0], rows_a, keys_a, values_a, allowed),
                group_update(current[1], rows_b, keys_b, values_b, allowed),
            )

        return lax.cond(first <= latest, compute, lambda current: current, states)

    return lax.fori_loop(0, length // step, inner, carry)


def finish_group(states, mix, gain):
    outputs = [state[0] / jnp.transpose(state[2])[:, :, None] for state in states]
    mixed = outputs[0] - mix[None, :, None] * outputs[1]
    normed = rms_scaled(mixed, gain) * HEAD_SCALE
    return normed.astype(jnp.bfloat16).reshape(mixed.shape[0], -1)


def per_device(
    resid,
    query_a,
    key_a,
    value_a,
    query_b,
    key_b,
    value_b,
    mix_a,
    mix_b,
    head_gain_a,
    head_gain_b,
    proj_a,
    proj_b,
    norm_gain,
    route_ids,
    route_weights,
    expert_gate,
    expert_up,
    expert_down,
):
    seq_rows = query_a.shape[0]
    sp_ways = lax.axis_size("sp")
    place = lax.axis_index("sp")
    positions = place * seq_rows + jnp.arange(seq_rows, dtype=jnp.int32)
    query_sets = ((query_a, query_b, positions),)

    def fold_keys(carry, pieces):
        return tuple(
            (set_update(states, queries, pieces) for states, queries in zip(carry, query_sets))
        )

    initial = tuple(
        (
            (empty_group(queries[0], value_a), empty_group(queries[1], value_b))
            for queries in query_sets
        )
    )
    results = fold_keys(initial, sent_together((key_a, value_a, key_b, value_b), "sp", 0, 2))
    finished = [
        (finish_group(states[0], mix_a, head_gain_a), finish_group(states[1], mix_b, head_gain_b))
        for states in results
    ]
    heads_out_a, heads_out_b = finished[0]
    width = resid.shape[1]
    tok_rows = resid.shape[0]
    top_count = route_ids.shape[1]
    capacity = 3 * top_count * tok_rows // (2 * sp_ways)
    own_slots = slot_numbers(route_ids, sp_ways, capacity)
    term = jnp.dot(heads_out_a, proj_a, preferred_element_type=jnp.float32)
    term = term + jnp.dot(heads_out_b, proj_b, preferred_element_type=jnp.float32)
    mixed = resid.astype(jnp.float32) + sent_and_summed(
        lax.optimization_barrier(term.astype(jnp.bfloat16))
        .astype(jnp.float32)
        .astype(jnp.bfloat16),
        "tp",
        0,
    )
    normed = rms_scaled(mixed, norm_gain).astype(jnp.bfloat16)
    lookup = jnp.arange(sp_ways * capacity, dtype=jnp.int32)[:, None]
    spread = jnp.zeros((sp_ways * capacity, tok_rows), jnp.float32)
    for which in range(top_count):
        spread = spread + (own_slots[:, which][None, :] == lookup).astype(jnp.float32)
    outgoing = jnp.dot(
        spread.astype(jnp.bfloat16), normed, preferred_element_type=jnp.float32
    ).astype(jnp.bfloat16)
    arrived = lax.all_to_all(
        outgoing.reshape(sp_ways, capacity, width), "sp", split_axis=0, concat_axis=0, tiled=True
    )
    piece = lax.all_gather(arrived.reshape(sp_ways * capacity, width), "tp", axis=0, tiled=True)
    gate = jnp.dot(piece, expert_gate[0], preferred_element_type=jnp.float32)
    upward = jnp.dot(piece, expert_up[0], preferred_element_type=jnp.float32)
    hidden = (jax.nn.silu(gate) * upward).astype(jnp.bfloat16)
    term = jnp.dot(hidden, expert_down[0], preferred_element_type=jnp.float32)
    summed = lax.psum_scatter(
        lax.optimization_barrier(term.astype(jnp.bfloat16))
        .astype(jnp.float32)
        .astype(jnp.bfloat16),
        "tp",
        scatter_dimension=0,
        tiled=True,
    )
    finished_rows = summed.reshape(sp_ways, capacity, width)
    back = lax.all_to_all(finished_rows, "sp", split_axis=0, concat_axis=0, tiled=True)
    picked = jnp.take(back.reshape(sp_ways * capacity, width), own_slots.reshape(-1), axis=0)
    picked = picked.reshape(tok_rows, top_count, width)
    output = mixed + jnp.sum(route_weights[:, :, None] * picked.astype(jnp.float32), axis=1)
    return output.astype(jnp.bfloat16)


def solution(mesh):
    placed = (
        P(("sp", "tp"), None),
        P("sp", "tp", None),
        P("sp", "tp", None),
        P("sp", "tp", None),
        P("sp", "tp", None),
        P("sp", "tp", None),
        P("sp", "tp", None),
        P("tp"),
        P("tp"),
        P(),
        P(),
        P("tp", None),
        P("tp", None),
        P(),
        P(("sp", "tp"), None),
        P(("sp", "tp"), None),
        P("sp", None, "tp"),
        P("sp", None, "tp"),
        P("sp", "tp", None),
    )
    return jax.shard_map(
        per_device, mesh=mesh, in_specs=placed, out_specs=P(("sp", "tp"), None), check_vma=False
    )
```

profile of v0, /device:TPU:1, one launch (start us, length us, event | category | flops | bytes accessed | tf_op | source)
XLA Modules:
  0.0 513.2 jit_solution(15753976325861860569)
XLA Ops:
  6.5 1.1 copy.36
  7.7 1.0 copy.37
  8.7 1.7 pad_maximum_fusion
  10.4 0.0 all-gather.3.cloned.1.call-update
  10.4 0.7 slice.45
  11.1 1.7 copy.38
  14.0 70.9 %all-gather.3.cloned.1.call-done = bf16[8192,1,384]{0,2,1:T(8,128)(2,1)} async-done(((bf16[512,1,384]{0,2,1:T(8,128)(2,1)}), bf16[8192,1,384]{0,2,1:T(8,128)(2,1)}) %all-gather.3.cloned.1.call-update) | async-done | bytes 6291472 | tf_op jit(solution)/shard_map/all_gather | solution.py:16
  84.9 4.7 fusion.100
  89.6 4.1 copy.39
  93.6 3.1 fusion.99
  96.9 0.0 copy-start.7
  96.9 22.8 %while.36 = (s32[]{:T(128)}, f32[512,1,128]{0,2,1:T(8,128)S(1)}, f32[1,512]{1,0:T(1,128)S(1)}, f32[1,512]{1,0:T(1,128)S(1)}, f32[512,1,128]{0,2,1:T(8,128)S(1)},...) while((s32[]{:T(128)}, f32[512,1,128]{0,2,1:T(8,128)S(1)}, ...), condition=%wide.region_11.12_spmd.clone, body=%wide.region_0.11_spmd.clone.sunk | while | flops 314184704 | bytes 15643357 | solution.py:118
  97.6 10.8 %conditional.3 = ((f32[512,1,128]{0,2,1:T(8,128)S(1)}, f32[1,512]{1,0:T(1,128)S(1)}, f32[1,512]{1,0:T(1,128)S(1)}, f32[512,1,128]{0,2,1:T(8,128)S(1)}, f32[1,512...) conditional(s32[]{:T(128)} %convert_element_type.133, ...), branch_computations={%region_1.0_spmd, %region_2.10_spmd} | conditional | flops 314184704 | bytes 15640814 | solution.py:116
  97.7 1.2 fusion.97
  98.9 0.0 copy-start.3
  98.9 1.1 fusion.96
  100.1 1.1 fusion.98
  101.2 1.2 fusion.95
  102.4 0.8 fusion.16
  103.2 1.2 fusion.9
  104.4 1.2 fusion.8
  105.7 1.3 fusion.7
  107.0 1.3 fusion.6
  119.7 0.1 multiply_reduce_fusion.2
  119.8 0.1 multiply_reduce_fusion.3
  119.8 0.0 copy-start.2
  119.8 0.0 copy-start.8
  119.9 1.9 fusion.74
  121.8 2.1 add_convert_fusion
  123.9 9.2 %all-to-all-start = ((bf16[16,32,2048]{2,1,0:T(8,128)(2,1)}), bf16[16,32,2048]{2,1,0:T(8,128)(2,1)}, u32[]{:S(2)}, u32[]{:S(2)}) async-start(bf16[16,32,2048]{2,1,0:T(8,128)(2,1)} %bitcast.147), calls=%async_computation | async-start | bytes 4194304 | tf_op jit(solution)/shard_map/all_to_all | solution.py:30
  133.0 0.0 all-gather.5.cloned.1.call-start
  133.1 0.1 copy.41
  133.2 0.1 reshape.243
  133.3 0.1 fusion.86
  133.4 0.1 reduce_window_sum.11
  133.5 0.2 select_reduce_fusion
  133.7 0.1 reduce_sum.106
  133.8 0.1 copy.42
  133.9 48.3 %all-to-all-done = bf16[16,32,2048]{2,1,0:T(8,128)(2,1)} async-done(((bf16[16,32,2048]{2,1,0:T(8,128)(2,1)}), bf16[16,32,2048]{2,1,0:T(8,128)(2,1)}, u32[]{:S(2)}, u32[]{:S(2)}) %all-to-all-start) | async-done | bytes 2097184 | tf_op jit(solution)/shard_map/all_to_all | solution.py:30
  182.2 2.0 convert_reduce_fusion
  184.2 0.1 multiply_reduce_fusion.1
  184.4 0.3 convolution_convert_fusion.1
  184.7 0.1 reshape.244
  184.8 175.7 %all_to_all.15 = bf16[16,6,2048]{2,1,0:T(8,128)(2,1)S(1)} all-to-all(bf16[16,6,2048]{2,1,0:T(8,128)(2,1)S(1)} %reshape.244), channel_id=1, replica_groups=mesh['sp'=16,'tp'=16] {'sp'}, dimensions={0} | all-to-all | bytes 786432 | tf_op jit(solution)/shard_map/all_to_all | solution.py:194
  360.5 0.9 reshape.245
  361.4 0.0 all-gather.5.cloned.1.call-update
  361.4 0.2 reduce-scatter.2.cloned.1.call-start
  361.7 42.4 %all-gather.5.cloned.1.call-done = bf16[1536,2048]{1,0:T(8,128)(2,1)} async-done(((bf16[96,2048]{1,0:T(8,128)(2,1)}), bf16[1536,2048]{1,0:T(8,128)(2,1)}) %all-gather.5.cloned.1.call-update) | async-done | bytes 6291472 | tf_op jit(solution)/shard_map/all_gather | solution.py:197
  404.1 8.1 %fusion.69 = f32[1536,384]{1,0:T(8,128)} fusion(bf16[1536,2048]{1,0:T(8,128)(2,1)} %all-gather.5.cloned.1.call-done, bf16[1,2048,384]{2,1,0:T(8,128)(2,1)} %param.39), kind=kOutput, calls=%fused_computation.100 | convolution fusion | flops 2415919104 | bytes 10223616 | tf_op jit(solution)/shard_map/dot_general | solution.py:198
  412.2 11.2 %convolution_convert_fusion = bf16[1536,2048]{1,0:T(8,128)(2,1)} fusion(bf16[1,384,2048]{2,1,0:T(8,128)(2,1)S(1)} %copy-done, bf16[1536,2048]{1,0:T(8,128)(2,1)} %all-gather.5.cloned.1.call-done, f32[1536,384]{1,0:T(8,128)} %fusion.69, bf16[1,2048,384]{2,1,0:T(8,128)(2,1)} %param.40), kind=kOutput, calls=%fused_computation.92 | convolution fusion | flops 4838522880 | bytes 18087936 | tf_op jit(solution)/shard_map/dot_general | solution.py:201
  423.4 0.0 reduce-scatter.2.cloned.1.call-update
  423.4 62.3 %reduce-scatter.2.cloned.1.call-done = bf16[96,2048]{1,0:T(8,128)(2,1)} async-done(((bf16[1536,2048]{1,0:T(8,128)(2,1)}), bf16[96,2048]{1,0:T(8,128)(2,1)}) %reduce-scatter.2.cloned.1.call-update) | async-done | bytes 393232 | tf_op jit(solution)/shard_map/reduce_scatter | solution.py:202
  485.7 1.9 reshape.246
  487.6 6.5 %all-to-all-start.2 = ((bf16[16,6,2048]{2,1,0:T(8,128)(2,1)}), bf16[16,6,2048]{2,1,0:T(8,128)(2,1)S(1)}, u32[]{:S(2)}, u32[]{:S(2)}) async-start(bf16[16,6,2048]{2,1,0:T(8,128)(2,1)} %reshape.246), calls=%async_computation.3 | async-start | bytes 1048576 | tf_op jit(solution)/shard_map/all_to_all | solution.py:211
  494.1 0.1 copy.44
  494.2 0.1 mul.249
  494.3 0.1 copy.43
  494.4 0.1 copy.40
  494.5 8.6 %all-to-all-done.2 = bf16[16,6,2048]{2,1,0:T(8,128)(2,1)S(1)} async-done(((bf16[16,6,2048]{2,1,0:T(8,128)(2,1)}), bf16[16,6,2048]{2,1,0:T(8,128)(2,1)S(1)}, u32[]{:S(2)}, u32[]{:S(2)}) %all-to-all-start.2) | async-done | bytes 393248 | tf_op jit(solution)/shard_map/all_to_all | solution.py:211
  503.2 0.1 reshape.247
  503.3 0.7 gather_fusion
  504.1 0.2 gather.7
  504.3 1.7 multiply_reduce_fusion
  506.0 0.7 add_convert_fusion.1
  (81 shorter events, 0.6 us)
Async XLA Ops:
  6.5 405.7 %copy-start = (bf16[1,384,2048]{2,1,0:T(8,128)(2,1)S(1)}, bf16[1,384,2048]{2,1,0:T(8,128)(2,1)}, u32[]{:S(2)}) copy-start(bf16[1,384,2048]{2,1,0:T(8,128)(2,1)} %param.41) | copy-start | bytes 4718596
  6.5 78.3 %all-gather.3.cloned.1.call-start = ((), (), s32[]{:S(2)}) async-start(), calls=%async_computation.4 | async-start | bytes 6684672 | tf_op jit(solution)/shard_map/all_gather | solution.py:16
  93.6 3.2 copy-start.9
  96.9 23.0 %copy-start.7 = (f32[128]{0:T(128)S(1)}, f32[128]{0:T(128)}, u32[]{:S(2)}) copy-start(f32[128]{0:T(128)} %param.32) | copy-start | bytes 1540
  98.9 2.3 copy-start.3
  119.8 1.9 copy-start.2
  119.8 1.9 copy-start.8
  123.9 9.2 %copy-start.4 = (s32[32,2]{0,1:T(2,128)S(1)}, s32[32,2]{0,1:T(2,128)}, u32[]{:S(2)}) copy-start(s32[32,2]{0,1:T(2,128)} %param.37) | copy-start | bytes 772
  123.9 60.3 %copy-start.1 = (bf16[32,2048]{1,0:T(8,128)(2,1)S(1)}, bf16[32,2048]{1,0:T(8,128)(2,1)}, u32[]{:S(2)}) copy-start(bf16[32,2048]{1,0:T(8,128)(2,1)} %param.23) | copy-start | bytes 393220
  123.9 58.3 %all-to-all-start = ((bf16[16,32,2048]{2,1,0:T(8,128)(2,1)}), bf16[16,32,2048]{2,1,0:T(8,128)(2,1)}, u32[]{:S(2)}, u32[]{:S(2)}) async-start(bf16[16,32,2048]{2,1,0:T(8,128)(2,1)} %bitcast.147), calls=%async_computation | async-start | bytes 4194304 | tf_op jit(solution)/shard_map/all_to_all | solution.py:30
  133.0 51.3 %copy-start.5 = (f32[2048]{0:T(1024)S(1)}, f32[2048]{0:T(1024)}, u32[]{:S(2)}) copy-start(f32[2048]{0:T(1024)} %param.36) | copy-start | bytes 24580
  133.0 271.0 %all-gather.5.cloned.1.call-start = ((), (), s32[]{:S(2)}) async-start(), calls=%async_computation.5 | async-start | bytes 6684672 | tf_op jit(solution)/shard_map/all_gather | solution.py:197
  361.4 124.3 %reduce-scatter.2.cloned.1.call-start = ((), (), s32[]{:S(2)}) async-start(), calls=%async_computation.6 | async-start | bytes 6684672 | tf_op jit(solution)/shard_map/reduce_scatter | solution.py:202
  423.4 71.0 %copy-start.6 = (f32[32,2]{0,1:T(2,128)S(1)}, f32[32,2]{0,1:T(2,128)}, u32[]{:S(2)}) copy-start(f32[32,2]{0,1:T(2,128)} %param.38) | copy-start | bytes 772
  487.6 15.5 %all-to-all-start.2 = ((bf16[16,6,2048]{2,1,0:T(8,128)(2,1)}), bf16[16,6,2048]{2,1,0:T(8,128)(2,1)S(1)}, u32[]{:S(2)}, u32[]{:S(2)}) async-start(bf16[16,6,2048]{2,1,0:T(8,128)(2,1)} %reshape.246), calls=%async_computation.3 | async-start | bytes 1048576 | tf_op jit(solution)/shard_map/all_to_all | solution.py:211
Sparse Core Ops, SparseCore 0:
  10.5 74.3 all-gather.2
  361.6 42.4 all-gather.4
  423.6 62.1 reduce-scatter.1
where the time goes:
time: 522 us; the launch traced here: 513 us
  waiting for transfers between devices  233 us (45%)
  blocking collectives  176 us (34%)
  matrix products  33.3 us (6%)
  local copies, waits for them, and re-layouts  21.2 us (4%)
  starting transfers between devices  15.9 us (3%)
  between operations  14.7 us (3%)
  loops' own time  12.1 us (2%)
  other arithmetic  7.62 us (1%)
    all_to_all x1, blocking collectives, per_device(): lax.all_to_all(outgoing.reshape(sp_ways, capacity, width), 'sp', split_ax...  176 us
    all_gather x1, waiting for transfers between devices, sent_together(): lax.all_gather(both, axis, axis=dim, tiled=True)  70.9 us
    reduce_scatter x1, waiting for transfers between devices, per_device(): lax.psum_scatter(lax.optimization_barrier(term.astype(jnp.bfloat16)).asty...  62.3 us
    all_to_all x1, waiting for transfers between devices, sent_and_summed(): lax.all_to_all(parts, axis, split_axis=0, concat_axis=0, tiled=True)  48.3 us
    all_gather x1, waiting for transfers between devices, per_device(): lax.all_gather(arrived.reshape(sp_ways * capacity, width), 'tp', axis=0,...  42.4 us
    another operation x1, loops' own time, set_update(): return lax.fori_loop(0, length // step, inner, carry)  11.6 us
    dot_general x1, matrix products, per_device(): term = jnp.dot(hidden, expert_down[0], preferred_element_type=jnp.float32)  11.2 us
  transfers between devices with their start and end apart: 5, of which 5 were waited for; matrix products, arithmetic and copies ran while one was open for 1% of the time, Pallas kernels for 0%

commit v1 on v0

v1 whole, which is shorter than its diff:
```python
import math

import jax
import jax.numpy as jnp
from jax import lax
from jax.experimental import pallas as pl
from jax.experimental.pallas import tpu as pltpu
from jax.sharding import PartitionSpec as P

EPS = 1e-06
NEG = -1e30
HEAD_SCALE = 1.0 - (0.8 - 0.6 * math.exp(-0.3))


def cut_along(value, dim, size):
    before, after = (value.shape[:dim], value.shape[dim + 1 :])
    return jnp.moveaxis(value.reshape(*before, size, -1, *after), dim, 0)


def sent_and_summed(value, axis, dim):
    parts = cut_along(value, dim, lax.axis_size(axis))
    arrived = lax.all_to_all(parts, axis, split_axis=0, concat_axis=0, tiled=True)
    return arrived.astype(jnp.float32).sum(axis=0)


def rms_scaled(values, gain):
    return values * lax.rsqrt(jnp.mean(values * values, axis=-1, keepdims=True) + EPS) * gain


def slot_numbers(route_rows, experts, capacity):
    count, top_count = route_rows.shape
    flat = route_rows.reshape(count * top_count)
    onehot = (flat[:, None] == jnp.arange(experts, dtype=jnp.int32)[None, :]).astype(jnp.int32)
    ranks = jnp.sum((jnp.cumsum(onehot, axis=0) - onehot) * onehot, axis=1)
    return (flat * capacity + ranks).reshape(count, top_count)


MESH = pl.DeviceIdType.MESH
LOG2E = 1.4426950408889634
PART = 128


def dot32(a, b):
    return jnp.dot(a, b, preferred_element_type=jnp.float32)


def attention_kernel(
    qa_ref, qb_ref, ka_ref, va_ref, kb_ref, vb_ref, mix_ref, gain_a_ref, gain_b_ref,
    out_ref,
    buf, qta, qtb, acc_a, acc_b, m_ref, l_ref, send_sem, recv_sem,
):
    place = lax.axis_index("sp")
    tp = lax.axis_index("tp")
    y, x = place // 4, place % 4
    half = buf.shape[2]

    def at(ox, oy):
        return ((y + oy + 4) % 4) * 4 + (x + ox + 4) % 4

    def spot(h, df, dg):
        return at(df, dg) if h == 0 else at(dg, df)

    barrier = pltpu.get_barrier_semaphore()
    for ox, oy in ((1, 0), (-1, 0), (0, 1), (0, -1)):
        pl.semaphore_signal(barrier, inc=1, device_id=(at(ox, oy), tp), device_id_type=MESH)

    va_t = jnp.transpose(va_ref[...])
    for h in range(2):
        cols = slice(h * half, (h + 1) * half)
        buf[place, h, :, 0:128] = ka_ref[cols, :]
        buf[place, h, 0:128, 128:384] = va_t[:, cols]
        buf[place, h, 128:192, 128:384] = kb_ref[:, cols]
        buf[place, h, 192:256, 128:384] = vb_ref[:, cols]

    pl.semaphore_wait(barrier, 4)

    def region(h, df, dg, part):
        ref = buf.at[spot(h, df, dg), h]
        return ref if part is None else ref.at[pl.ds(part * PART, PART)]

    def copy(h, number, df, dg, part, to_f, to_g):
        ref = region(h, df, dg, part)
        return pltpu.make_async_remote_copy(
            src_ref=ref,
            dst_ref=ref,
            send_sem=send_sem.at[h * 20 + number],
            recv_sem=recv_sem.at[h * 20 + number],
            device_id=(spot(h, to_f, to_g), tp),
            device_id_type=MESH,
        )

    moves = {
        0: (0, 0, None, 1, 0), 1: (0, 0, None, -1, 0),
        2: (0, 0, None, 0, 1), 3: (0, 0, None, 0, -1),
        4: (-1, 0, 0, 1, 0), 5: (1, 0, 1, -1, 0),
        6: (-1, 0, None, 0, 1), 7: (-1, 0, None, 0, -1),
        8: (1, 0, None, 0, 1), 9: (1, 0, None, 0, -1),
        10: (2, 0, None, 0, 1), 11: (2, 0, None, 0, -1),
        12: (0, -1, 0, 0, 1), 13: (0, 1, 1, 0, -1),
        14: (-1, -1, 0, 0, 1), 15: (-1, 1, 1, 0, -1),
        16: (1, -1, 0, 0, 1), 17: (1, 1, 1, 0, -1),
        18: (2, -1, 0, 0, 1), 19: (2, 1, 1, 0, -1),
    }

    def start(*numbers):
        for number in numbers:
            for h in range(2):
                copy(h, number, *moves[number]).start()

    def arrive(number, *then):
        df, dg, part, to_f, to_g = moves[number]
        for h in range(2):
            copy(h, number, df - to_f, dg - to_g, part, to_f, to_g).wait_recv()
            for follow in then:
                copy(h, follow, *moves[follow]).start()

    start(0, 1, 2, 3)

    qa_t = jnp.transpose(qa_ref[...])
    zero_a = jnp.zeros((64, half), jnp.bfloat16)
    zero_b = jnp.zeros((32, half), jnp.bfloat16)
    for h in range(2):
        cols = slice(h * half, (h + 1) * half)
        qta[h, 0:64, :] = qa_t[0:64, cols]
        qta[h, 64:128, :] = zero_a
        qta[2 + h, 0:64, :] = zero_a
        qta[2 + h, 64:128, :] = qa_t[64:128, cols]
        qtb[h, 0:32, :] = qb_ref[0:32, cols]
        qtb[h, 32:64, :] = zero_b
        qtb[2 + h, 0:32, :] = zero_b
        qtb[2 + h, 32:64, :] = qb_ref[32:64, cols]
    acc_a[...] = jnp.zeros_like(acc_a)
    acc_b[...] = jnp.zeros_like(acc_b)
    m_ref[...] = jnp.full_like(m_ref, NEG)
    l_ref[...] = jnp.zeros_like(l_ref)

    def fold(index, slot, scores, v_parts, acc, factor, offsets):
        if offsets is not None:
            query_pos = lax.rem(index, 2) * half + lax.broadcasted_iota(jnp.int32, (half, half), 1)
            scores = [
                jnp.where(
                    lax.broadcasted_iota(jnp.int32, (half, half), 0) + first <= query_pos, s, NEG
                )
                for s, first in zip(scores, offsets)
            ]
        top = jnp.maximum(
            jnp.max(scores[0], axis=0, keepdims=True), jnp.max(scores[1], axis=0, keepdims=True)
        )
        old = m_ref[slot]
        fresh = jnp.maximum(old, top)
        scale = jnp.exp2((old - fresh) * factor)
        weights = [jnp.exp2((s - fresh) * factor) for s in scores]
        m_ref[slot] = fresh
        l_ref[slot] = (
            l_ref[slot] * scale
            + jnp.sum(weights[0], axis=0, keepdims=True)
            + jnp.sum(weights[1], axis=0, keepdims=True)
        )
        acc[index] = (
            acc[index] * scale
            + dot32(v_parts[0], weights[0].astype(jnp.bfloat16))
            + dot32(v_parts[1], weights[1].astype(jnp.bfloat16))
        )

    def block(source, offsets):
        k_b = [jnp.transpose(buf[source, h, 128:192, 128:384]) for h in range(2)]

        def tile(index, carry):
            q_a, q_b = qta[index], qtb[index]
            fold(
                index, index,
                [dot32(buf[source, h, :, 0:128], q_a) for h in range(2)],
                [buf[source, h, 0:128, 128:384] for h in range(2)],
                acc_a, LOG2E / 8.0, offsets,
            )
            fold(
                index, index + 4,
                [dot32(k_b[h], q_b) for h in range(2)],
                [buf[source, h, 192:256, 128:384] for h in range(2)],
                acc_b, LOG2E / math.sqrt(32.0), offsets,
            )
            return carry

        lax.fori_loop(0, 4, tile, 0)

    def group(offsets):
        def step(number, carry):
            ox, oy = jnp.int32(0), jnp.int32(0)
            for which, (dx, dy) in enumerate(offsets):
                ox = jnp.where(number == which, dx, ox)
                oy = jnp.where(number == which, dy, oy)
            source = at(ox, oy)

            @pl.when(source < place)
            def _():
                block(source, None)

            return carry

        lax.fori_loop(0, len(offsets), step, 0)

    block(place, (0, half))
    arrive(0, 4, 6, 7)
    arrive(1, 5, 8, 9)
    arrive(2, 12)
    arrive(3, 13)
    group(((-1, 0), (0, -1), (1, 0), (0, 1)))
    arrive(4)
    arrive(5, 10, 11)
    arrive(6, 14)
    arrive(7, 15)
    arrive(8, 16)
    arrive(9, 17)
    arrive(12)
    arrive(13)
    group(((-1, -1), (1, -1), (-1, 1), (1, 1), (2, 0), (0, 2)))
    arrive(10, 18)
    arrive(11, 19)
    for number in (14, 15, 16, 17):
        arrive(number)
    group(((2, -1), (-1, 2), (1, 2), (2, 1)))
    arrive(18)
    arrive(19)
    group(((2, 2),))

    for h in range(2):
        for acc, base, which, gain, first in (
            (acc_a, 0, 0, gain_a_ref, 0), (acc_b, 4, 1, gain_b_ref, 128),
        ):
            one = acc[h] / l_ref[base + h]
            two = acc[2 + h] / l_ref[base + 2 + h]
            mixed = one - mix_ref[which] * two
            mixed = mixed * lax.rsqrt(jnp.mean(mixed * mixed, axis=0, keepdims=True) + EPS)
            rows = jnp.transpose(mixed) * gain[...] * HEAD_SCALE
            out_ref[h * half : (h + 1) * half, first : first + rows.shape[1]] = rows.astype(
                jnp.bfloat16
            )
    for number in range(20):
        for h in range(2):
            copy(h, number, *moves[number]).wait_send()


def attention(query_a, key_a, value_a, query_b, key_b, value_b, mix_a, mix_b, gain_a, gain_b):
    rows = query_a.shape[0]
    vmem = pl.BlockSpec(memory_space=pltpu.VMEM)
    return pl.pallas_call(
        attention_kernel,
        out_shape=jax.ShapeDtypeStruct((rows, 192), jnp.bfloat16),
        in_specs=[vmem] * 6 + [pl.BlockSpec(memory_space=pltpu.SMEM)] + [vmem] * 2,
        out_specs=vmem,
        scratch_shapes=[
            pltpu.VMEM((16, 2, 256, 384), jnp.bfloat16),
            pltpu.VMEM((4, 128, 256), jnp.bfloat16),
            pltpu.VMEM((4, 64, 256), jnp.bfloat16),
            pltpu.VMEM((4, 128, 256), jnp.float32),
            pltpu.VMEM((4, 64, 256), jnp.float32),
            pltpu.VMEM((8, 1, 256), jnp.float32),
            pltpu.VMEM((8, 1, 256), jnp.float32),
            pltpu.SemaphoreType.DMA((40,)),
            pltpu.SemaphoreType.DMA((40,)),
        ],
        compiler_params=pltpu.CompilerParams(collective_id=0, has_side_effects=True),
    )(
        query_a[:, 0, :], query_b[:, 0, :].T, key_a[:, 0, :], value_a[:, 0, :],
        key_b[:, 0, :].T, value_b[:, 0, :].T,
        jnp.concatenate([mix_a, mix_b]), gain_a[None, :], gain_b[None, :],
    )


def per_device(
    resid,
    query_a,
    key_a,
    value_a,
    query_b,
    key_b,
    value_b,
    mix_a,
    mix_b,
    head_gain_a,
    head_gain_b,
    proj_a,
    proj_b,
    norm_gain,
    route_ids,
    route_weights,
    expert_gate,
    expert_up,
    expert_down,
):
    sp_ways = lax.axis_size("sp")
    heads_out = attention(
        query_a, key_a, value_a, query_b, key_b, value_b, mix_a, mix_b, head_gain_a, head_gain_b
    )
    width = resid.shape[1]
    tok_rows = resid.shape[0]
    top_count = route_ids.shape[1]
    capacity = 3 * top_count * tok_rows // (2 * sp_ways)
    own_slots = slot_numbers(route_ids, sp_ways, capacity)
    term = jnp.dot(heads_out[:, :128], proj_a, preferred_element_type=jnp.float32)
    term = term + jnp.dot(heads_out[:, 128:], proj_b, preferred_element_type=jnp.float32)
    mixed = resid.astype(jnp.float32) + sent_and_summed(
        lax.optimization_barrier(term.astype(jnp.bfloat16))
        .astype(jnp.float32)
        .astype(jnp.bfloat16),
        "tp",
        0,
    )
    normed = rms_scaled(mixed, norm_gain).astype(jnp.bfloat16)
    lookup = jnp.arange(sp_ways * capacity, dtype=jnp.int32)[:, None]
    spread = jnp.zeros((sp_ways * capacity, tok_rows), jnp.float32)
    for which in range(top_count):
        spread = spread + (own_slots[:, which][None, :] == lookup).astype(jnp.float32)
    outgoing = jnp.dot(
        spread.astype(jnp.bfloat16), normed, preferred_element_type=jnp.float32
    ).astype(jnp.bfloat16)
    arrived = lax.all_to_all(
        outgoing.reshape(sp_ways, capacity, width), "sp", split_axis=0, concat_axis=0, tiled=True
    )
    piece = lax.all_gather(arrived.reshape(sp_ways * capacity, width), "tp", axis=0, tiled=True)
    gate = jnp.dot(piece, expert_gate[0], preferred_element_type=jnp.float32)
    upward = jnp.dot(piece, expert_up[0], preferred_element_type=jnp.float32)
    hidden = (jax.nn.silu(gate) * upward).astype(jnp.bfloat16)
    term = jnp.dot(hidden, expert_down[0], preferred_element_type=jnp.float32)
    summed = lax.psum_scatter(
        lax.optimization_barrier(term.astype(jnp.bfloat16))
        .astype(jnp.float32)
        .astype(jnp.bfloat16),
        "tp",
        scatter_dimension=0,
        tiled=True,
    )
    finished_rows = summed.reshape(sp_ways, capacity, width)
    back = lax.all_to_all(finished_rows, "sp", split_axis=0, concat_axis=0, tiled=True)
    picked = jnp.take(back.reshape(sp_ways * capacity, width), own_slots.reshape(-1), axis=0)
    picked = picked.reshape(tok_rows, top_count, width)
    output = mixed + jnp.sum(route_weights[:, :, None] * picked.astype(jnp.float32), axis=1)
    return output.astype(jnp.bfloat16)


def solution(mesh):
    placed = (
        P(("sp", "tp"), None),
        P("sp", "tp", None),
        P("sp", "tp", None),
        P("sp", "tp", None),
        P("sp", "tp", None),
        P("sp", "tp", None),
        P("sp", "tp", None),
        P("tp"),
        P("tp"),
        P(),
        P(),
        P("tp", None),
        P("tp", None),
        P(),
        P(("sp", "tp"), None),
        P(("sp", "tp"), None),
        P("sp", None, "tp"),
        P("sp", None, "tp"),
        P("sp", "tp", None),
    )
    return jax.shard_map(
        per_device, mesh=mesh, in_specs=placed, out_specs=P(("sp", "tp"), None), check_vma=False
    )
```

time: 522 us -> 316 us (0.61); the launches traced: 513 us -> 313 us
  blocking collectives: 176 us -> 33.9 us
  waiting for transfers between devices: 233 us -> 162 us
  Pallas kernels: 0 us -> 50.3 us
  local copies, waits for them, and re-layouts: 21.2 us -> 4.8 us
  loops' own time: 12.1 us -> 0 us
  matrix products: 33.3 us -> 23 us
    all_to_all x1, blocking collectives: 176 us -> 33.9 us  [per_device(): lax.all_to_all(outgoing.reshape(sp_ways, capacity, width), 'sp', split_ax...]
    all_gather x1 -> x0, waiting for transfers between devices: 70.9 us -> none  [sent_together(): lax.all_gather(both, axis, axis=dim, tiled=True)]
    pallas_call x0 -> x1, Pallas kernels: none -> 50.3 us  [attention(): pl.pallas_call(attention_kernel, out_shape=jax.ShapeDtypeStruct((rows, 19...]
    another operation x17 -> x0, loops' own time: 12.1 us -> none  [the longest x1 11.6 us: set_update(): return lax.fori_loop(0, length // step, inner, carry)]
    dot_general x10 -> x2, matrix products: 13.7 us -> 3.85 us  [the longest x1 2 us: per_device(): jnp.dot(heads_out[:, 128:], proj_b, preferred_element_type=jnp.float32)]
    slice x3 -> x0, local copies, waits for them, and re-layouts: 8.39 us -> none  [the longest x2 7.74 us: sent_together(): lax.slice_in_dim(result, at, at + a.shape[along], axis=along)]
    unnamed x24 -> x18, local copies, waits for them, and re-layouts: 8.08 us -> 0.21 us
  transfers between devices with their start and end apart: 5 -> 4, of which waited for: 5 -> 4; matrix products, arithmetic and copies ran while one was open for 1% -> 0% of each run, Pallas kernels for 0% -> 0%
where the time goes in v1:
time: 316 us; the launch traced here: 313 us
  waiting for transfers between devices  162 us (51%)
  Pallas kernels  50.3 us (16%)
  blocking collectives  33.9 us (11%)
  matrix products  23 us (7%)
  starting transfers between devices  18.8 us (6%)
  between operations  15 us (5%)
  other arithmetic  5.58 us (2%)
  local copies, waits for them, and re-layouts  4.8 us (2%)
    reduce_scatter x1, waiting for transfers between devices, per_device(): lax.psum_scatter(lax.optimization_barrier(term.astype(jnp.bfloat16)).asty...  62.3 us
    pallas_call x1, Pallas kernels, attention(): pl.pallas_call(attention_kernel, out_shape=jax.ShapeDtypeStruct((rows, 19...  50.3 us
    all_to_all x1, waiting for transfers between devices, sent_and_summed(): lax.all_to_all(parts, axis, split_axis=0, concat_axis=0, tiled=True)  48.3 us
    all_gather x1, waiting for transfers between devices, per_device(): lax.all_gather(arrived.reshape(sp_ways * capacity, width), 'tp', axis=0,...  42.4 us
    all_to_all x1, blocking collectives, per_device(): lax.all_to_all(outgoing.reshape(sp_ways, capacity, width), 'sp', split_ax...  33.9 us
    all_to_all x1, starting transfers between devices, sent_and_summed(): lax.all_to_all(parts, axis, split_axis=0, concat_axis=0, tiled=True)  12.1 us
    dot_general x1, matrix products, per_device(): term = jnp.dot(hidden, expert_down[0], preferred_element_type=jnp.float32)  10.7 us
    all_to_all x1, waiting for transfers between devices, per_device(): lax.all_to_all(finished_rows, 'sp', split_axis=0, concat_axis=0, tiled=True)  8.65 us
  transfers between devices with their start and end apart: 4, of which 4 were waited for; matrix products, arithmetic and copies ran while one was open for 0% of the time, Pallas kernels for 0%

profile of v1, /device:TPU:1, one launch (start us, length us, event | category | flops | bytes accessed | tf_op | source)
XLA Modules:
  0.0 313.0 jit_solution(10485993588444840236)
XLA Ops:
  6.5 0.0 copy-start
  8.0 0.6 pad_maximum_fusion.mix_ref
  8.5 50.3 %shard_map.181 = bf16[512,192]{1,0:T(8,128)(2,1)} custom-call(bf16[512,128]{1,0:T(8,128)(2,1)} %bitcast.41, bf16[64,512]{1,0:T(8,128)(2,1)} %bitcast.44, bf16[512,128]{1,0:T(8,128)(2,1)} %bitcast.42, bf16[512,128]{1,0:T(8,128)(2,1)} %bitcast.43, bf16[64,512]{1,0:T(8,128)(2,1)} %bitcast.45, bf16[64,512]{1,0:T(8,128)(2,1)} %bitcast.46, ...), custom_call_target="tpu_custom_call" | custom-call | tf_op jit(solution)/shard_map/pallas_call | solution.py:246
  58.9 0.0 copy-start.2
  58.9 0.0 copy-start.3
  58.9 1.9 fusion.10
  60.7 0.0 copy-done.2
  60.7 0.0 copy-done.3
  60.8 2.0 add_convert_fusion
  62.7 0.0 copy-start.4
  62.8 0.0 copy-start.1
  62.8 12.1 %all-to-all-start = ((bf16[16,32,2048]{2,1,0:T(8,128)(2,1)}), bf16[16,32,2048]{2,1,0:T(8,128)(2,1)}, u32[]{:S(2)}, u32[]{:S(2)}) async-start(bf16[16,32,2048]{2,1,0:T(8,128)(2,1)} %bitcast.40), calls=%async_computation | async-start | bytes 4194304 | tf_op jit(solution)/shard_map/all_to_all | solution.py:22
  74.8 0.0 copy-start.5
  74.8 0.0 all-gather.2.cloned.1.call-start
  74.9 0.0 copy-done.4
  74.9 0.1 copy.27
  75.0 0.1 reshape.76
  75.1 0.1 fusion.12
  75.2 0.1 reduce_window_sum.11
  75.3 0.2 select_reduce_fusion
  75.4 0.1 reduce_sum.42
  75.6 0.1 copy.28
  75.7 48.3 %all-to-all-done = bf16[16,32,2048]{2,1,0:T(8,128)(2,1)} async-done(((bf16[16,32,2048]{2,1,0:T(8,128)(2,1)}), bf16[16,32,2048]{2,1,0:T(8,128)(2,1)}, u32[]{:S(2)}, u32[]{:S(2)}) %all-to-all-start) | async-done | bytes 2097184 | tf_op jit(solution)/shard_map/all_to_all | solution.py:22
  124.0 2.0 convert_reduce_fusion
  126.0 0.0 copy-done.1
  126.0 0.2 multiply_reduce_fusion.1
  126.2 0.0 copy-done.5
  126.2 0.3 convolution_convert_fusion.1
  126.5 0.1 reshape.77
  126.6 33.9 %all_to_all.15 = bf16[16,6,2048]{2,1,0:T(8,128)(2,1)S(1)} all-to-all(bf16[16,6,2048]{2,1,0:T(8,128)(2,1)S(1)} %reshape.77), channel_id=1, replica_groups=mesh['sp'=16,'tp'=16] {'sp'}, dimensions={0} | all-to-all | bytes 786432 | tf_op jit(solution)/shard_map/all_to_all | solution.py:317
  160.5 0.9 reshape.78
  161.3 0.0 all-gather.2.cloned.1.call-update
  161.4 0.0 copy-start.7
  161.4 0.2 reduce-scatter.2.cloned.1.call-start
  161.6 42.4 %all-gather.2.cloned.1.call-done = bf16[1536,2048]{1,0:T(8,128)(2,1)} async-done(((bf16[96,2048]{1,0:T(8,128)(2,1)}), bf16[1536,2048]{1,0:T(8,128)(2,1)}) %all-gather.2.cloned.1.call-update) | async-done | bytes 6291472 | tf_op jit(solution)/shard_map/all_gather | solution.py:320
  204.0 8.1 %fusion.3 = f32[1536,384]{1,0:T(8,128)} fusion(bf16[1536,2048]{1,0:T(8,128)(2,1)} %all-gather.2.cloned.1.call-done, bf16[1,2048,384]{2,1,0:T(8,128)(2,1)} %param.35), kind=kOutput, calls=%fused_computation.9 | convolution fusion | flops 2415919104 | bytes 10223616 | tf_op jit(solution)/shard_map/dot_general | solution.py:321
  212.1 0.0 copy-done
  212.1 0.0 copy-done.7
  212.1 10.7 %convolution_convert_fusion = bf16[1536,2048]{1,0:T(8,128)(2,1)} fusion(bf16[1,384,2048]{2,1,0:T(8,128)(2,1)S(1)} %copy-done, bf16[1536,2048]{1,0:T(8,128)(2,1)} %all-gather.2.cloned.1.call-done, f32[1536,384]{1,0:T(8,128)} %fusion.3, bf16[1,2048,384]{2,1,0:T(8,128)(2,1)S(1)} %copy-done.7), kind=kOutput, calls=%fused_computation.1 | convolution fusion | flops 4838522880 | bytes 18087936 | tf_op jit(solution)/shard_map/dot_general | solution.py:324
  222.9 0.0 copy-start.6
  222.9 0.0 reduce-scatter.2.cloned.1.call-update
  222.9 62.3 %reduce-scatter.2.cloned.1.call-done = bf16[96,2048]{1,0:T(8,128)(2,1)} async-done(((bf16[1536,2048]{1,0:T(8,128)(2,1)}), bf16[96,2048]{1,0:T(8,128)(2,1)}) %reduce-scatter.2.cloned.1.call-update) | async-done | bytes 393232 | tf_op jit(solution)/shard_map/reduce_scatter | solution.py:325
  285.2 1.9 reshape.79
  287.1 6.5 %all-to-all-start.2 = ((bf16[16,6,2048]{2,1,0:T(8,128)(2,1)}), bf16[16,6,2048]{2,1,0:T(8,128)(2,1)S(1)}, u32[]{:S(2)}, u32[]{:S(2)}) async-start(bf16[16,6,2048]{2,1,0:T(8,128)(2,1)} %reshape.79), calls=%async_computation.3 | async-start | bytes 1048576 | tf_op jit(solution)/shard_map/all_to_all | solution.py:334
  293.6 0.1 copy.30
  293.7 0.1 mul.68
  293.8 0.1 copy.29
  293.9 0.0 copy-done.6
  293.9 0.1 copy.26
  294.0 8.7 %all-to-all-done.2 = bf16[16,6,2048]{2,1,0:T(8,128)(2,1)S(1)} async-done(((bf16[16,6,2048]{2,1,0:T(8,128)(2,1)}), bf16[16,6,2048]{2,1,0:T(8,128)(2,1)S(1)}, u32[]{:S(2)}, u32[]{:S(2)}) %all-to-all-start.2) | async-done | bytes 393248 | tf_op jit(solution)/shard_map/all_to_all | solution.py:334
  302.7 0.1 reshape.80
  302.8 0.7 gather_fusion
  303.5 0.2 gather.7
  303.7 1.7 multiply_reduce_fusion
  305.5 0.7 add_convert_fusion.1
  (6 shorter events, 0.0 us)
Async XLA Ops:
  6.5 205.6 %copy-start = (bf16[1,384,2048]{2,1,0:T(8,128)(2,1)S(1)}, bf16[1,384,2048]{2,1,0:T(8,128)(2,1)}, u32[]{:S(2)}) copy-start(bf16[1,384,2048]{2,1,0:T(8,128)(2,1)} %param.37) | copy-start | bytes 4718596
  58.9 1.9 copy-start.2
  58.9 1.9 copy-start.3
  62.7 12.1 %copy-start.4 = (s32[32,2]{0,1:T(2,128)S(1)}, s32[32,2]{0,1:T(2,128)}, u32[]{:S(2)}) copy-start(s32[32,2]{0,1:T(2,128)} %param.33) | copy-start | bytes 772
  62.8 63.2 %copy-start.1 = (bf16[32,2048]{1,0:T(8,128)(2,1)S(1)}, bf16[32,2048]{1,0:T(8,128)(2,1)}, u32[]{:S(2)}) copy-start(bf16[32,2048]{1,0:T(8,128)(2,1)} %param.19) | copy-start | bytes 393220
  62.8 61.2 %all-to-all-start = ((bf16[16,32,2048]{2,1,0:T(8,128)(2,1)}), bf16[16,32,2048]{2,1,0:T(8,128)(2,1)}, u32[]{:S(2)}, u32[]{:S(2)}) async-start(bf16[16,32,2048]{2,1,0:T(8,128)(2,1)} %bitcast.40), calls=%async_computation | async-start | bytes 4194304 | tf_op jit(solution)/shard_map/all_to_all | solution.py:22
  74.8 51.3 %copy-start.5 = (f32[2048]{0:T(1024)S(1)}, f32[2048]{0:T(1024)}, u32[]{:S(2)}) copy-start(f32[2048]{0:T(1024)} %param.32) | copy-start | bytes 24580
  74.8 129.2 %all-gather.2.cloned.1.call-start = ((), (), s32[]{:S(2)}) async-start(), calls=%async_computation.4 | async-start | bytes 6684672 | tf_op jit(solution)/shard_map/all_gather | solution.py:320
  161.4 50.7 %copy-start.7 = (bf16[1,2048,384]{2,1,0:T(8,128)(2,1)S(1)}, bf16[1,2048,384]{2,1,0:T(8,128)(2,1)}, u32[]{:S(2)}) copy-start(bf16[1,2048,384]{2,1,0:T(8,128)(2,1)} %param.36) | copy-start | bytes 4718596
  161.4 123.8 %reduce-scatter.2.cloned.1.call-start = ((), (), s32[]{:S(2)}) async-start(), calls=%async_computation.5 | async-start | bytes 6684672 | tf_op jit(solution)/shard_map/reduce_scatter | solution.py:325
  222.9 71.0 %copy-start.6 = (f32[32,2]{0,1:T(2,128)S(1)}, f32[32,2]{0,1:T(2,128)}, u32[]{:S(2)}) copy-start(f32[32,2]{0,1:T(2,128)} %param.34) | copy-start | bytes 772
  287.1 15.6 %all-to-all-start.2 = ((bf16[16,6,2048]{2,1,0:T(8,128)(2,1)}), bf16[16,6,2048]{2,1,0:T(8,128)(2,1)S(1)}, u32[]{:S(2)}, u32[]{:S(2)}) async-start(bf16[16,6,2048]{2,1,0:T(8,128)(2,1)} %reshape.79), calls=%async_computation.3 | async-start | bytes 1048576 | tf_op jit(solution)/shard_map/all_to_all | solution.py:334
Sparse Core Ops, SparseCore 0:
  161.5 42.4 all-gather.1
  223.0 62.1 reduce-scatter.1

commit v2 on v1

--- a/solution.py
+++ b/solution.py
@@ -10,17 +10,6 @@
 EPS = 1e-06
 NEG = -1e30
 HEAD_SCALE = 1.0 - (0.8 - 0.6 * math.exp(-0.3))
-
-
-def cut_along(value, dim, size):
-    before, after = (value.shape[:dim], value.shape[dim + 1 :])
-    return jnp.moveaxis(value.reshape(*before, size, -1, *after), dim, 0)
-
-
-def sent_and_summed(value, axis, dim):
-    parts = cut_along(value, dim, lax.axis_size(axis))
-    arrived = lax.all_to_all(parts, axis, split_axis=0, concat_axis=0, tiled=True)
-    return arrived.astype(jnp.float32).sum(axis=0)
 
 
 def rms_scaled(values, gain):
@@ -265,6 +254,311 @@
         key_b[:, 0, :].T, value_b[:, 0, :].T,
         jnp.concatenate([mix_a, mix_b]), gain_a[None, :], gain_b[None, :],
     )
+
+
+def tp_place():
+    tp = lax.axis_index("tp")
+    return lax.axis_index("sp"), tp // 2, tp % 2
+
+
+def meet_tp(sp, z, core):
+    barrier = pltpu.get_barrier_semaphore()
+    for peer in (((z + 1) % 8) * 2 + core, ((z + 7) % 8) * 2 + core, z * 2 + 1 - core):
+        pl.semaphore_signal(barrier, inc=1, device_id=(sp, peer), device_id_type=MESH)
+    pl.semaphore_wait(barrier, 3)
+
+
+class Exchange:
+    def __init__(self, pbuf, other, stage, landed, pair_send, pair_recv, ring_send, ring_recv):
+        self.sp, self.z, self.core = tp_place()
+        self.pbuf, self.other, self.stage, self.landed = pbuf, other, stage, landed
+        self.pair_sems, self.ring_sems = (pair_send, pair_recv), (ring_send, ring_recv)
+        self.rows = pbuf.shape[1] // 2
+
+    def chip(self, offset):
+        return (self.z + offset + 8) % 8
+
+    def pair_copy(self, offset):
+        chip = self.chip(offset)
+        return pltpu.make_async_remote_copy(
+            src_ref=self.pbuf.at[chip * 2 + 1 - self.core],
+            dst_ref=self.other.at[chip],
+            send_sem=self.pair_sems[0].at[offset + 3],
+            recv_sem=self.pair_sems[1].at[offset + 3],
+            device_id=(self.sp, self.z * 2 + 1 - self.core),
+            device_id_type=MESH,
+        )
+
+    def ring_copy(self, way, half, distance):
+        number = way * 8 + half * 4 + distance - 1
+        return pltpu.make_async_remote_copy(
+            src_ref=self.stage.at[way, half, distance - 1],
+            dst_ref=self.landed.at[way, half, distance - 1],
+            send_sem=self.ring_sems[0].at[number],
+            recv_sem=self.ring_sems[1].at[number],
+            device_id=(self.sp, self.chip(1 - 2 * way) * 2 + self.core),
+            device_id_type=MESH,
+        )
+
+    def mine(self, offset, half):
+        chip = self.chip(offset)
+        rows = slice(half * self.rows, (half + 1) * self.rows)
+        own = self.pbuf[chip * 2 + self.core, rows, :].astype(jnp.float32)
+        return own + self.other[chip, rows, :].astype(jnp.float32)
+
+    def send(self, way, half, distance):
+        offset = distance * (1 - 2 * way)
+        total = self.mine(4 if distance == 4 else offset, half)
+        if distance < (4 if half == way else 3):
+            self.ring_copy(way, half, distance + 1).wait_recv()
+            total = total + self.landed[way, half, distance].astype(jnp.float32)
+        self.stage[way, half, distance - 1] = total.astype(jnp.bfloat16)
+        self.ring_copy(way, half, distance).start()
+
+    def last(self, half):
+        total = self.mine(0, half)
+        for way in range(2):
+            self.ring_copy(way, half, 1).wait_recv()
+            total = total + self.landed[way, half, 0].astype(jnp.float32)
+        return total
+
+    def finish(self):
+        for offset in range(-3, 5):
+            self.pair_copy(offset).wait_send()
+        for way in range(2):
+            for half in range(2):
+                for distance in range(1, 5 if half == way else 4):
+                    self.ring_copy(way, half, distance).wait_send()
+
+
+def exchange_scratch(rows, width):
+    return [
+        pltpu.VMEM((16, rows, width), jnp.bfloat16),
+        pltpu.VMEM((8, rows, width), jnp.bfloat16),
+        pltpu.VMEM((2, 2, 4, rows // 2, width), jnp.bfloat16),
+        pltpu.VMEM((2, 2, 4, rows // 2, width), jnp.bfloat16),
+        pltpu.SemaphoreType.DMA((8,)),
+        pltpu.SemaphoreType.DMA((8,)),
+        pltpu.SemaphoreType.DMA((16,)),
+        pltpu.SemaphoreType.DMA((16,)),
+    ]
+
+
+def project_kernel(
+    heads_ref, proj_a_ref, proj_b_ref, resid_ref, gain_ref, spread_ref, mixed_ref, out_ref,
+    pbuf, other, stage, landed, pair_send, pair_recv, ring_send, ring_recv,
+):
+    sp, z, core = tp_place()
+    ex = Exchange(pbuf, other, stage, landed, pair_send, pair_recv, ring_send, ring_recv)
+    for first in range(0, 2048, 512):
+        cols = slice(first, first + 512)
+        term = dot32(heads_ref[:, 0:128], proj_a_ref[:, cols])
+        term = term + dot32(heads_ref[:, 128:192], proj_b_ref[:, cols])
+        pbuf[:, :, cols] = term.astype(jnp.bfloat16).reshape(16, 32, 512)
+    meet_tp(sp, z, core)
+    order = (4, 3, -3, 2, -2, 1, -1, 0)
+    for offset in order:
+        ex.pair_copy(offset).start()
+    ex.pair_copy(4).wait_recv()
+    ex.send(0, 0, 4)
+    ex.send(1, 1, 4)
+    for distance in (3, 2, 1):
+        ex.pair_copy(distance).wait_recv()
+        ex.pair_copy(-distance).wait_recv()
+        if distance == 3:
+            ex.send(0, 1, 3)
+            ex.send(1, 0, 3)
+        ex.send(0, 0, distance)
+        ex.send(1, 1, distance)
+        if distance < 3:
+            ex.send(0, 1, distance)
+            ex.send(1, 0, distance)
+    ex.pair_copy(0).wait_recv()
+    for half in range(2):
+        rows = slice(half * 16, half * 16 + 16)
+        mixed_ref[rows, :] = resid_ref[rows, :].astype(jnp.float32) + ex.last(half)
+    normed = rms_scaled(mixed_ref[...], gain_ref[...]).astype(jnp.bfloat16)
+    out_ref[...] = dot32(spread_ref[...], normed).astype(jnp.bfloat16)
+    ex.finish()
+
+
+def project(heads_out, proj_a, proj_b, resid, norm_gain, spread):
+    rows, width = resid.shape
+    vmem = pl.BlockSpec(memory_space=pltpu.VMEM)
+    return pl.pallas_call(
+        project_kernel,
+        out_shape=(
+            jax.ShapeDtypeStruct((rows, width), jnp.float32),
+            jax.ShapeDtypeStruct((spread.shape[0], width), jnp.bfloat16),
+        ),
+        in_specs=[vmem] * 6,
+        out_specs=(vmem, vmem),
+        scratch_shapes=exchange_scratch(rows, width),
+        compiler_params=pltpu.CompilerParams(collective_id=1, has_side_effects=True),
+    )(heads_out, proj_a, proj_b, resid, norm_gain[None, :], spread)
+
+
+def expert_kernel(
+    rows_ref, gate_hbm, up_hbm, down_hbm, out_ref,
+    xbuf, gate, up, down, w_sem, ag_send, ag_recv, share_send, share_recv,
+    pbuf, other, stage, landed, pair_send, pair_recv, ring_send, ring_recv,
+):
+    sp, z, core = tp_place()
+    ex = Exchange(pbuf, other, stage, landed, pair_send, pair_recv, ring_send, ring_recv)
+    loads = [
+        pltpu.make_async_copy(src, dst, w_sem.at[i])
+        for i, (src, dst) in enumerate(((gate_hbm, gate), (up_hbm, up), (down_hbm, down)))
+    ]
+    for load in loads:
+        load.start()
+    xbuf[z * 2 + core] = rows_ref[...]
+    meet_tp(sp, z, core)
+    part = rows_ref.shape[0] // 2
+
+    def shard(offset, half):
+        chip = ex.chip(offset)
+        return xbuf.at[chip * 2 + core, pl.ds(half * part, part)]
+
+    def ag_copy(way, half, distance, arriving=False):
+        sign = 1 - 2 * way
+        away = distance + 1 if arriving else distance
+        offset = 4 if away == 4 else -sign * away
+        here = rows_ref.at[pl.ds(half * part, part)] if away == 0 else shard(offset, half)
+        number = way * 8 + half * 4 + distance
+        return pltpu.make_async_remote_copy(
+            src_ref=here,
+            dst_ref=shard(offset, half),
+            send_sem=ag_send.at[number],
+            recv_sem=ag_recv.at[number],
+            device_id=(sp, ex.chip(sign) * 2 + core),
+            device_id_type=MESH,
+        )
+
+    def share_copy(offset, half, arriving=False):
+        chip = ex.chip(offset)
+        there = xbuf.at[chip * 2 + (1 - core if arriving else core), pl.ds(half * part, part)]
+        here = there
+        if offset == 0 and not arriving:
+            here = rows_ref.at[pl.ds(half * part, part)]
+        number = (offset + 3) * 2 + half
+        return pltpu.make_async_remote_copy(
+            src_ref=here,
+            dst_ref=there,
+            send_sem=share_send.at[number],
+            recv_sem=share_recv.at[number],
+            device_id=(sp, z * 2 + 1 - core),
+            device_id_type=MESH,
+        )
+
+    def came(way, half, distance):
+        ag_copy(way, half, distance - 1, arriving=True).wait_recv()
+        if distance < (4 if half == way else 3):
+            ag_copy(way, half, distance).start()
+        offset = 4 if distance == 4 else -distance * (1 - 2 * way)
+        share_copy(offset, half).start()
+
+    def feed(offset):
+        for half in range(2):
+            share_copy(offset, half, arriving=True).wait_recv()
+
+    def experts(first, count):
+        def step(number, carry):
+            chip = ex.chip(first - 2 * first * number)
+            piece = xbuf[pl.ds(chip * 2, 2)].reshape(4 * part, xbuf.shape[2])
+            gated = dot32(piece, gate[0])
+            upward = dot32(piece, up[0])
+            hidden = (jax.nn.silu(gated) * upward).astype(jnp.bfloat16)
+            for begin in range(0, xbuf.shape[2], 512):
+                cols = slice(begin, begin + 512)
+                term = dot32(hidden, down[0, :, cols]).astype(jnp.bfloat16)
+                pbuf[pl.ds(chip * 2, 2), :, cols] = term.reshape(2, 2 * part, 512)
+            return carry
+
+        lax.fori_loop(0, count, step, 0)
+
+    for way in range(2):
+        ag_copy(way, way, 0).start()
+        ag_copy(way, 1 - way, 0).start()
+    for half in range(2):
+        share_copy(0, half).start()
+    for distance in (1, 2, 3):
+        came(0, 0, distance)
+        came(1, 1, distance)
+        came(0, 1, distance)
+        came(1, 0, distance)
+        if distance == 1:
+            for load in loads:
+                load.wait()
+            feed(0)
+            experts(0, 1)
+            ex.pair_copy(0).start()
+        else:
+            feed(1 - distance)
+            feed(distance - 1)
+            experts(distance - 1, 2)
+            ex.pair_copy(1 - distance).start()
+            ex.pair_copy(distance - 1).start()
+    feed(-3)
+    feed(3)
+    experts(3, 2)
+    ex.pair_copy(-3).start()
+    ex.pair_copy(3).start()
+    came(0, 0, 4)
+    came(1, 1, 4)
+    ex.pair_copy(3).wait_recv()
+    ex.send(0, 1, 3)
+    ex.pair_copy(-3).wait_recv()
+    ex.send(1, 0, 3)
+    feed(4)
+    experts(4, 1)
+    ex.pair_copy(4).start()
+    for offset in (2, -2, 1, -1, 0, 4):
+        ex.pair_copy(offset).wait_recv()
+    ex.send(0, 0, 4)
+    ex.send(1, 1, 4)
+    for distance in (3, 2, 1):
+        if distance < 3:
+            ex.send(0, 1, distance)
+            ex.send(1, 0, distance)
+        ex.send(0, 0, distance)
+        ex.send(1, 1, distance)
+    for half in range(2):
+        out_ref[half * part : (half + 1) * part, :] = ex.last(half).astype(jnp.bfloat16)
+    ex.finish()
+    for way in range(2):
+        for half in range(2):
+            for distance in range(4 if half == way else 3):
+                ag_copy(way, half, distance).wait_send()
+    for offset in range(-3, 5):
+        for half in range(2):
+            share_copy(offset, half).wait_send()
+
+
+def run_experts(rows, gate, up, down):
+    count, width = rows.shape
+    vmem = pl.BlockSpec(memory_space=pltpu.VMEM)
+    anywhere = pl.BlockSpec(memory_space=pl.ANY)
+    return pl.pallas_call(
+        expert_kernel,
+        out_shape=jax.ShapeDtypeStruct((count, width), jnp.bfloat16),
+        in_specs=[vmem, anywhere, anywhere, anywhere],
+        out_specs=vmem,
+        scratch_shapes=[
+            pltpu.VMEM((16, count, width), jnp.bfloat16),
+            pltpu.VMEM(gate.shape, gate.dtype),
+            pltpu.VMEM(up.shape, up.dtype),
+            pltpu.VMEM(down.shape, down.dtype),
+            pltpu.SemaphoreType.DMA((3,)),
+            pltpu.SemaphoreType.DMA((16,)),
+            pltpu.SemaphoreType.DMA((16,)),
+            pltpu.SemaphoreType.DMA((16,)),
+            pltpu.SemaphoreType.DMA((16,)),
+        ]
+        + exchange_scratch(count, width),
+        compiler_params=pltpu.CompilerParams(
+            collective_id=2, has_side_effects=True, vmem_limit_bytes=60 * 1024 * 1024
+        ),
+    )(rows, gate, up, down)
 
 
 def per_device(
@@ -297,38 +591,18 @@
     top_count = route_ids.shape[1]
     capacity = 3 * top_count * tok_rows // (2 * sp_ways)
     own_slots = slot_numbers(route_ids, sp_ways, capacity)
-    term = jnp.dot(heads_out[:, :128], proj_a, preferred_element_type=jnp.float32)
-    term = term + jnp.dot(heads_out[:, 128:], proj_b, preferred_element_type=jnp.float32)
-    mixed = resid.astype(jnp.float32) + sent_and_summed(
-        lax.optimization_barrier(term.astype(jnp.bfloat16))
-        .astype(jnp.float32)
-        .astype(jnp.bfloat16),
-        "tp",
-        0,
-    )
-    normed = rms_scaled(mixed, norm_gain).astype(jnp.bfloat16)
     lookup = jnp.arange(sp_ways * capacity, dtype=jnp.int32)[:, None]
     spread = jnp.zeros((sp_ways * capacity, tok_rows), jnp.float32)
     for which in range(top_count):
         spread = spread + (own_slots[:, which][None, :] == lookup).astype(jnp.float32)
-    outgoing = jnp.dot(
-        spread.astype(jnp.bfloat16), normed, preferred_element_type=jnp.float32
-    ).astype(jnp.bfloat16)
+    mixed, outgoing = project(
+        heads_out, proj_a, proj_b, resid, norm_gain, spread.astype(jnp.bfloat16)
+    )
     arrived = lax.all_to_all(
         outgoing.reshape(sp_ways, capacity, width), "sp", split_axis=0, concat_axis=0, tiled=True
     )
-    piece = lax.all_gather(arrived.reshape(sp_ways * capacity, width), "tp", axis=0, tiled=True)
-    gate = jnp.dot(piece, expert_gate[0], preferred_element_type=jnp.float32)
-    upward = jnp.dot(piece, expert_up[0], preferred_element_type=jnp.float32)
-    hidden = (jax.nn.silu(gate) * upward).astype(jnp.bfloat16)
-    term = jnp.dot(hidden, expert_down[0], preferred_element_type=jnp.float32)
-    summed = lax.psum_scatter(
-        lax.optimization_barrier(term.astype(jnp.bfloat16))
-        .astype(jnp.float32)
-        .astype(jnp.bfloat16),
-        "tp",
-        scatter_dimension=0,
-        tiled=True,
+    summed = run_experts(
+        arrived.reshape(sp_ways * capacity, width), expert_gate, expert_up, expert_down
     )
     finished_rows = summed.reshape(sp_ways, capacity, width)
     back = lax.all_to_all(finished_rows, "sp", split_axis=0, concat_axis=0, tiled=True)

time: 316 us -> 212 us (0.67)
  waiting for transfers between devices: 162 us -> 9.55 us
  Pallas kernels: 50.3 us -> 152 us
  matrix products: 23 us -> 0 us
  starting transfers between devices: 18.8 us -> 3.57 us
  between operations: 15 us -> 1.43 us
    pallas_call x0 -> x2, Pallas kernels: none -> 102 us  [the longest x1 73.5 us: run_experts(): pl.pallas_call(expert_kernel, out_shape=jax.ShapeDtypeStruct((count, widt...]
    reduce_scatter x1 -> x0, waiting for transfers between devices: 62.3 us -> none  [per_device(): lax.psum_scatter(lax.optimization_barrier(term.astype(jnp.bfloat16)).asty...]
    all_to_all x1 -> x0, waiting for transfers between devices: 48.3 us -> none  [sent_and_summed(): lax.all_to_all(parts, axis, split_axis=0, concat_axis=0, tiled=True)]
    all_gather x1 -> x0, waiting for transfers between devices: 42.4 us -> none  [per_device(): lax.all_gather(arrived.reshape(sp_ways * capacity, width), 'tp', axis=0,...]
    dot_general x5 -> x0, matrix products: 23 us -> none  [the longest x1 10.7 us: per_device(): term = jnp.dot(hidden, expert_down[0], preferred_element_type=jnp.float32)]
    all_to_all x1 -> x0, starting transfers between devices: 12.1 us -> none  [sent_and_summed(): lax.all_to_all(parts, axis, split_axis=0, concat_axis=0, tiled=True)]
  transfers between devices with their start and end apart: 4 -> 1, of which waited for: 4 -> 1; matrix products, arithmetic and copies ran while one was open for 0% -> 0% of each run, Pallas kernels for 0% -> 0%
where the time goes in v2:
time: 212 us; the launch traced here: 211 us
  Pallas kernels  152 us (72%)
  blocking collectives  32.7 us (15%)
  waiting for transfers between devices  9.55 us (5%)
  local copies, waits for them, and re-layouts  6.44 us (3%)
  other arithmetic  4.76 us (2%)
  starting transfers between devices  3.57 us (2%)
    pallas_call x1, Pallas kernels, run_experts(): pl.pallas_call(expert_kernel, out_shape=jax.ShapeDtypeStruct((count, widt...  73.5 us
    pallas_call x1, Pallas kernels, attention(): pl.pallas_call(attention_kernel, out_shape=jax.ShapeDtypeStruct((rows, 19...  50.2 us
    all_to_all x1, blocking collectives, per_device(): lax.all_to_all(outgoing.reshape(sp_ways, capacity, width), 'sp', split_ax...  32.7 us
    pallas_call x1, Pallas kernels, project(): pl.pallas_call(project_kernel, out_shape=(jax.ShapeDtypeStruct((rows, wid...  28.4 us
    all_to_all x1, waiting for transfers between devices, per_device(): lax.all_to_all(finished_rows, 'sp', split_axis=0, concat_axis=0, tiled=True)  9.55 us
  transfers between devices with their start and end apart: 1, of which 1 were waited for; matrix products, arithmetic and copies ran while one was open for 0% of the time, Pallas kernels for 0%

profile of v2, /device:TPU:1, one launch (start us, length us, event | category | flops | bytes accessed | tf_op | source)
XLA Modules:
  0.0 210.6 jit_solution(15197255349952696885)
XLA Ops:
  1.3 0.8 copy.26
  2.1 0.1 eq.45
  2.2 0.1 fusion
  2.2 0.1 reduce_window_sum.11
  2.3 0.2 select_reduce_fusion
  2.5 0.1 reduce_sum.23
  2.6 0.1 copy.27
  2.7 0.7 compare_and_fusion
  3.4 0.7 pad_maximum_fusion.mix_ref
  4.1 0.6 add_convert_fusion.1.spread_ref
  4.7 50.2 %shard_map.181.heads_ref = bf16[512,192]{1,0:T(8,128)(2,1)} custom-call(bf16[512,128]{1,0:T(8,128)(2,1)} %bitcast.25, bf16[64,512]{1,0:T(8,128)(2,1)} %bitcast.28, bf16[512,128]{1,0:T(8,128)(2,1)} %bitcast.26, bf16[512,128]{1,0:T(8,128)(2,1)} %bitcast.27, bf16[64,512]{1,0:T(8,128)(2,1)} %bitcast.29, bf16[64,512]{1,0:T(8,128)(2,1)} %bitcast.30, ...), custom_call_target="tpu_custom_call" | custom-call | tf_op jit(solution)/shard_map/pallas_call | solution.py:235
  54.9 28.4 %shard_map.182 = (f32[32,2048]{1,0:T(8,128)}, bf16[96,2048]{1,0:T(8,128)(2,1)}) custom-call(bf16[512,192]{1,0:T(8,128)(2,1)} %shard_map.181.heads_ref, bf16[128,2048]{1,0:T(8,128)(2,1)} %proj_a_ref.1, bf16[64,2048]{1,0:T(8,128)(2,1)} %proj_b_ref.1, bf16[32,2048]{1,0:T(8,128)(2,1)} %resid_ref.1, f32[1,2048]{1,0:T(1,128)} %bitcast.31, ...), custom_call_target="tpu_custom_call" | custom-call | tf_op jit(solution)/shard_map/pallas_call | solution.py:388
  83.4 1.1 reshape.61
  84.5 32.7 %all_to_all.10 = bf16[16,6,2048]{2,1,0:T(8,128)(2,1)S(1)} all-to-all(bf16[16,6,2048]{2,1,0:T(8,128)(2,1)S(1)} %reshape.61), channel_id=1, replica_groups=mesh['sp'=16,'tp'=16] {'sp'}, dimensions={0} | all-to-all | bytes 786432 | tf_op jit(solution)/shard_map/all_to_all | solution.py:601
  117.2 0.9 reshape.62.rows_ref
  118.1 73.5 %shard_map.183 = bf16[96,2048]{1,0:T(8,128)(2,1)} custom-call(bf16[96,2048]{1,0:T(8,128)(2,1)} %reshape.62.rows_ref, bf16[1,2048,384]{2,1,0:T(8,128)(2,1)} %gate_hbm.1, bf16[1,2048,384]{2,1,0:T(8,128)(2,1)} %up_hbm.1, bf16[1,384,2048]{2,1,0:T(8,128)(2,1)} %down_hbm.1), custom_call_target="tpu_custom_call" | custom-call | tf_op jit(solution)/shard_map/pallas_call | solution.py:541
  191.6 0.0 copy-start.1
  191.6 0.0 copy-start.2
  191.7 1.9 reshape.63
  193.6 3.6 %all-to-all-start.1 = ((bf16[16,6,2048]{2,1,0:T(8,128)(2,1)}), bf16[16,6,2048]{2,1,0:T(8,128)(2,1)S(1)}, u32[]{:S(2)}, u32[]{:S(2)}) async-start(bf16[16,6,2048]{2,1,0:T(8,128)(2,1)} %reshape.63), calls=%async_computation.1 | async-start | bytes 1048576 | tf_op jit(solution)/shard_map/all_to_all | solution.py:608
  197.2 0.0 copy-done.1
  197.2 0.1 copy.30
  197.3 0.1 mul.35
  197.4 0.1 copy.29
  197.5 0.0 copy-done.2
  197.5 0.1 copy.28
  197.6 9.5 %all-to-all-done.1 = bf16[16,6,2048]{2,1,0:T(8,128)(2,1)S(1)} async-done(((bf16[16,6,2048]{2,1,0:T(8,128)(2,1)}), bf16[16,6,2048]{2,1,0:T(8,128)(2,1)S(1)}, u32[]{:S(2)}, u32[]{:S(2)}) %all-to-all-start.1) | async-done | bytes 393248 | tf_op jit(solution)/shard_map/all_to_all | solution.py:608
  207.1 0.1 reshape.64
  207.3 0.0 copy-start
  207.3 0.7 gather_fusion
  208.0 0.2 gather.7
  208.2 1.7 multiply_reduce_fusion
  209.9 0.0 copy-done
  210.0 0.7 add_convert_fusion
  (4 shorter events, 0.0 us)
Async XLA Ops:
  191.6 5.5 %copy-start.1 = (s32[32,2]{0,1:T(2,128)S(1)}, s32[32,2]{0,1:T(2,128)}, u32[]{:S(2)}) copy-start(s32[32,2]{0,1:T(2,128)} %param.33) | copy-start | bytes 772
  191.6 5.8 %copy-start.2 = (f32[32,2]{0,1:T(2,128)S(1)}, f32[32,2]{0,1:T(2,128)}, u32[]{:S(2)}) copy-start(f32[32,2]{0,1:T(2,128)} %param.34) | copy-start | bytes 772
  193.6 13.6 %all-to-all-start.1 = ((bf16[16,6,2048]{2,1,0:T(8,128)(2,1)}), bf16[16,6,2048]{2,1,0:T(8,128)(2,1)S(1)}, u32[]{:S(2)}, u32[]{:S(2)}) async-start(bf16[16,6,2048]{2,1,0:T(8,128)(2,1)} %reshape.63), calls=%async_computation.1 | async-start | bytes 1048576 | tf_op jit(solution)/shard_map/all_to_all | solution.py:608
  207.3 2.7 %copy-start = (f32[32,2048]{1,0:T(8,128)S(1)}, f32[32,2048]{1,0:T(8,128)}, u32[]{:S(2)}) copy-start(f32[32,2048]{1,0:T(8,128)} %get-tuple-element.7) | copy-start | bytes 786436

commit v3 on v2

--- a/solution.py
+++ b/solution.py
@@ -16,17 +16,10 @@
     return values * lax.rsqrt(jnp.mean(values * values, axis=-1, keepdims=True) + EPS) * gain
 
 
-def slot_numbers(route_rows, experts, capacity):
-    count, top_count = route_rows.shape
-    flat = route_rows.reshape(count * top_count)
-    onehot = (flat[:, None] == jnp.arange(experts, dtype=jnp.int32)[None, :]).astype(jnp.int32)
-    ranks = jnp.sum((jnp.cumsum(onehot, axis=0) - onehot) * onehot, axis=1)
-    return (flat * capacity + ranks).reshape(count, top_count)
-
-
 MESH = pl.DeviceIdType.MESH
 LOG2E = 1.4426950408889634
 PART = 128
+CHUNK = 64
 
 
 def dot32(a, b):
@@ -34,10 +27,12 @@
 
 
 def attention_kernel(
-    qa_ref, qb_ref, ka_ref, va_ref, kb_ref, vb_ref, mix_ref, gain_a_ref, gain_b_ref,
+    qa_ref, qb_ref, ka_ref, va_ref, kb_ref, vb_ref, mix_a_ref, mix_b_ref, gain_a_ref, gain_b_ref,
     out_ref,
-    buf, qta, qtb, acc_a, acc_b, m_ref, l_ref, send_sem, recv_sem,
+    buf, qta, qtb, k_b, s_even, s_odd, p_even, p_odd, acc_a, acc_b, m_ref, l_ref,
+    send_sem, recv_sem,
 ):
+    s_refs, p_refs = (s_even, s_odd), (p_even, p_odd)
     place = lax.axis_index("sp")
     tp = lax.axis_index("tp")
     y, x = place // 4, place % 4
@@ -123,102 +118,94 @@
     m_ref[...] = jnp.full_like(m_ref, NEG)
     l_ref[...] = jnp.zeros_like(l_ref)
 
-    def fold(index, slot, scores, v_parts, acc, factor, offsets):
-        if offsets is not None:
-            query_pos = lax.rem(index, 2) * half + lax.broadcasted_iota(jnp.int32, (half, half), 1)
-            scores = [
-                jnp.where(
-                    lax.broadcasted_iota(jnp.int32, (half, half), 0) + first <= query_pos, s, NEG
-                )
-                for s, first in zip(scores, offsets)
-            ]
-        top = jnp.maximum(
-            jnp.max(scores[0], axis=0, keepdims=True), jnp.max(scores[1], axis=0, keepdims=True)
-        )
+    def score(number, source, offsets):
+        index, group, place_in = number // 2, number % 2, number % 2
+        top = None
+        for h in range(2):
+            keys = k_b[h] if group else buf[source, h, :, 0:128]
+            found = dot32(keys, qtb[index] if group else qta[index])
+            if offsets is not None:
+                query_pos = (index % 2) * half + lax.broadcasted_iota(jnp.int32, (half, half), 1)
+                key_pos = offsets[h] + lax.broadcasted_iota(jnp.int32, (half, half), 0)
+                found = jnp.where(key_pos <= query_pos, found, NEG)
+            s_refs[place_in][h * half : (h + 1) * half, :] = found
+            most = jnp.max(found.reshape(half // 8, 8, half), axis=0)
+            top = most if top is None else jnp.maximum(top, most)
+        return jnp.max(top, axis=0, keepdims=True)
+
+    def soften(number, top):
+        index, group = number // 2, number % 2
+        slot, factor = index + 4 * group, (LOG2E / math.sqrt(32.0) if group else LOG2E / 8.0)
         old = m_ref[slot]
         fresh = jnp.maximum(old, top)
         scale = jnp.exp2((old - fresh) * factor)
-        weights = [jnp.exp2((s - fresh) * factor) for s in scores]
         m_ref[slot] = fresh
-        l_ref[slot] = (
-            l_ref[slot] * scale
-            + jnp.sum(weights[0], axis=0, keepdims=True)
-            + jnp.sum(weights[1], axis=0, keepdims=True)
-        )
-        acc[index] = (
-            acc[index] * scale
-            + dot32(v_parts[0], weights[0].astype(jnp.bfloat16))
-            + dot32(v_parts[1], weights[1].astype(jnp.bfloat16))
-        )
+        sums = l_ref[slot] * scale
+        for first in range(0, 2 * half, CHUNK):
+            rows = slice(first, first + CHUNK)
+            weights = jnp.exp2((s_refs[group][rows, :] - fresh) * factor)
+            sums = sums + jnp.sum(weights.reshape(CHUNK // 8, 8, half), axis=0)
+            p_refs[group][rows, :] = weights.astype(jnp.bfloat16)
+        l_ref[slot] = sums
+        return scale
+
+    def gather(number, source, scale):
+        index, group = number // 2, number % 2
+        acc, rows = (acc_b, slice(192, 256)) if group else (acc_a, slice(0, 128))
+        added = dot32(buf[source, 0, rows, 128:384], p_refs[group][0:half, :])
+        added = added + dot32(buf[source, 1, rows, 128:384], p_refs[group][half : 2 * half, :])
+        acc[index] = acc[index] * scale + added
 
     def block(source, offsets):
-        k_b = [jnp.transpose(buf[source, h, 128:192, 128:384]) for h in range(2)]
-
-        def tile(index, carry):
-            q_a, q_b = qta[index], qtb[index]
-            fold(
-                index, index,
-                [dot32(buf[source, h, :, 0:128], q_a) for h in range(2)],
-                [buf[source, h, 0:128, 128:384] for h in range(2)],
-                acc_a, LOG2E / 8.0, offsets,
-            )
-            fold(
-                index, index + 4,
-                [dot32(k_b[h], q_b) for h in range(2)],
-                [buf[source, h, 192:256, 128:384] for h in range(2)],
-                acc_b, LOG2E / math.sqrt(32.0), offsets,
-            )
-            return carry
-
-        lax.fori_loop(0, 4, tile, 0)
-
-    def group(offsets):
-        def step(number, carry):
-            ox, oy = jnp.int32(0), jnp.int32(0)
-            for which, (dx, dy) in enumerate(offsets):
-                ox = jnp.where(number == which, dx, ox)
-                oy = jnp.where(number == which, dy, oy)
-            source = at(ox, oy)
-
-            @pl.when(source < place)
-            def _():
-                block(source, None)
-
-            return carry
-
-        lax.fori_loop(0, len(offsets), step, 0)
+        for h in range(2):
+            k_b[h] = jnp.transpose(buf[source, h, 128:192, 128:384])
+        top = score(0, source, offsets)
+        for number in range(8):
+            later = score(number + 1, source, offsets) if number < 7 else None
+            gather(number, source, soften(number, top))
+            top = later
+
+    plan = (
+        ((-1, 0), ()), ((0, -1), (4, 5)), ((1, 0), ()), ((0, 1), (6, 7)), ((-1, -1), ()),
+        ((1, -1), (8, 9)), ((-1, 1), ()), ((1, 1), ()), ((2, 0), (10, 11, 12, 13)), ((0, 2), ()),
+        ((2, -1), (14, 15)), ((-1, 2), ()), ((2, 1), (16, 17)), ((1, 2), ()), ((2, 2), (18, 19)),
+    )
+    follow = {5: (10, 11), 6: (14,), 7: (15,), 8: (16,), 9: (17,), 10: (18,), 11: (19,)}
+
+    def step(number, carry):
+        ox, oy = jnp.int32(0), jnp.int32(0)
+        for which, ((dx, dy), events) in enumerate(plan):
+            ox = jnp.where(number == which, dx, ox)
+            oy = jnp.where(number == which, dy, oy)
+            if events:
+
+                @pl.when(number == which)
+                def _(events=events):
+                    for event in events:
+                        arrive(event, *follow.get(event, ()))
+
+        source = at(ox, oy)
+
+        @pl.when(source < place)
+        def _():
+            block(source, None)
+
+        return carry
 
     block(place, (0, half))
     arrive(0, 4, 6, 7)
     arrive(1, 5, 8, 9)
     arrive(2, 12)
     arrive(3, 13)
-    group(((-1, 0), (0, -1), (1, 0), (0, 1)))
-    arrive(4)
-    arrive(5, 10, 11)
-    arrive(6, 14)
-    arrive(7, 15)
-    arrive(8, 16)
-    arrive(9, 17)
-    arrive(12)
-    arrive(13)
-    group(((-1, -1), (1, -1), (-1, 1), (1, 1), (2, 0), (0, 2)))
-    arrive(10, 18)
-    arrive(11, 19)
-    for number in (14, 15, 16, 17):
-        arrive(number)
-    group(((2, -1), (-1, 2), (1, 2), (2, 1)))
-    arrive(18)
-    arrive(19)
-    group(((2, 2),))
+    lax.fori_loop(0, len(plan), step, 0)
 
     for h in range(2):
-        for acc, base, which, gain, first in (
-            (acc_a, 0, 0, gain_a_ref, 0), (acc_b, 4, 1, gain_b_ref, 128),
+        for acc, base, mix, gain, first in (
+            (acc_a, 0, mix_a_ref, gain_a_ref, 0), (acc_b, 4, mix_b_ref, gain_b_ref, 128),
         ):
-            one = acc[h] / l_ref[base + h]
-            two = acc[2 + h] / l_ref[base + 2 + h]
-            mixed = one - mix_ref[which] * two
+            one = acc[h] / jnp.sum(l_ref[base + h], axis=0, keepdims=True)
+            two = acc[2 + h] / jnp.sum(l_ref[base + 2 + h], axis=0, keepdims=True)
+            mixed = one - mix[0] * two
             mixed = mixed * lax.rsqrt(jnp.mean(mixed * mixed, axis=0, keepdims=True) + EPS)
             rows = jnp.transpose(mixed) * gain[...] * HEAD_SCALE
             out_ref[h * half : (h + 1) * half, first : first + rows.shape[1]] = rows.astype(
@@ -235,16 +222,21 @@
     return pl.pallas_call(
         attention_kernel,
         out_shape=jax.ShapeDtypeStruct((rows, 192), jnp.bfloat16),
-        in_specs=[vmem] * 6 + [pl.BlockSpec(memory_space=pltpu.SMEM)] + [vmem] * 2,
+        in_specs=[vmem] * 6 + [pl.BlockSpec(memory_space=pltpu.SMEM)] * 2 + [vmem] * 2,
         out_specs=vmem,
         scratch_shapes=[
             pltpu.VMEM((16, 2, 256, 384), jnp.bfloat16),
             pltpu.VMEM((4, 128, 256), jnp.bfloat16),
             pltpu.VMEM((4, 64, 256), jnp.bfloat16),
+            pltpu.VMEM((2, 256, 64), jnp.bfloat16),
+            pltpu.VMEM((512, 256), jnp.float32),
+            pltpu.VMEM((512, 256), jnp.float32),
+            pltpu.VMEM((512, 256), jnp.bfloat16),
+            pltpu.VMEM((512, 256), jnp.bfloat16),
             pltpu.VMEM((4, 128, 256), jnp.float32),
             pltpu.VMEM((4, 64, 256), jnp.float32),
             pltpu.VMEM((8, 1, 256), jnp.float32),
-            pltpu.VMEM((8, 1, 256), jnp.float32),
+            pltpu.VMEM((8, 8, 256), jnp.float32),
             pltpu.SemaphoreType.DMA((40,)),
             pltpu.SemaphoreType.DMA((40,)),
         ],
@@ -252,7 +244,7 @@
     )(
         query_a[:, 0, :], query_b[:, 0, :].T, key_a[:, 0, :], value_a[:, 0, :],
         key_b[:, 0, :].T, value_b[:, 0, :].T,
-        jnp.concatenate([mix_a, mix_b]), gain_a[None, :], gain_b[None, :],
+        mix_a, mix_b, gain_a[None, :], gain_b[None, :],
     )
 
 
@@ -261,11 +253,14 @@
     return lax.axis_index("sp"), tp // 2, tp % 2
 
 
-def meet_tp(sp, z, core):
+def meet(sp, z, core):
+    tp = z * 2 + core
     barrier = pltpu.get_barrier_semaphore()
-    for peer in (((z + 1) % 8) * 2 + core, ((z + 7) % 8) * 2 + core, z * 2 + 1 - core):
-        pl.semaphore_signal(barrier, inc=1, device_id=(sp, peer), device_id_type=MESH)
-    pl.semaphore_wait(barrier, 3)
+    peers = [(sp, ((z + 1) % 8) * 2 + core), (sp, ((z + 7) % 8) * 2 + core), (sp, tp + 1 - 2 * core)]
+    peers += [((sp + delta) % 16, tp) for delta in range(1, 16)]
+    for peer in peers:
+        pl.semaphore_signal(barrier, inc=1, device_id=peer, device_id_type=MESH)
+    pl.semaphore_wait(barrier, len(peers))
 
 
 class Exchange:
@@ -344,76 +339,110 @@
     ]
 
 
-def project_kernel(
-    heads_ref, proj_a_ref, proj_b_ref, resid_ref, gain_ref, spread_ref, mixed_ref, out_ref,
-    pbuf, other, stage, landed, pair_send, pair_recv, ring_send, ring_recv,
+SLAB = 8
+
+
+def slab_copy(slabs, landing, delta, send_sem, recv_sem, arriving=False):
+    sp, tp = lax.axis_index("sp"), lax.axis_index("tp")
+    there = (sp + delta) % 16
+    return pltpu.make_async_remote_copy(
+        src_ref=slabs.at[there],
+        dst_ref=landing.at[(sp + 16 - delta) % 16 if arriving else sp],
+        send_sem=send_sem.at[delta],
+        recv_sem=recv_sem.at[delta],
+        device_id=(there, tp),
+        device_id_type=MESH,
+    )
+
+
+def chosen_slots(ids_ref):
+    tokens = ids_ref.shape[1]
+    expert = lax.broadcasted_iota(jnp.int32, (16, tokens), 0)
+    named = [(expert == ids_ref[r : r + 1, :]).astype(jnp.float32) for r in range(2)]
+    earlier = lax.broadcasted_iota(jnp.int32, (tokens, tokens), 0)
+    earlier = (earlier < lax.broadcasted_iota(jnp.int32, (tokens, tokens), 1)).astype(jnp.bfloat16)
+    before = dot32((named[0] + named[1]).astype(jnp.bfloat16), earlier)
+    slots = lax.broadcasted_iota(jnp.int32, (16 * SLAB, tokens), 0)
+    result = []
+    for r in range(2):
+        rank = jnp.sum(named[r] * before, axis=0, keepdims=True).astype(jnp.int32)
+        result.append((slots == ids_ref[r : r + 1, :] * SLAB + rank).astype(jnp.bfloat16))
+    return result
+
+
+def packing(rows, capacity):
+    shape = (rows, rows // capacity * SLAB)
+    row = lax.broadcasted_iota(jnp.int32, shape, 0)
+    column = lax.broadcasted_iota(jnp.int32, shape, 1)
+    used = column % SLAB < capacity
+    return (used & (row == column // SLAB * capacity + column % SLAB)).astype(jnp.bfloat16)
+
+
+def unpacking(rows, capacity):
+    shape = (rows // capacity * SLAB, rows)
+    row = lax.broadcasted_iota(jnp.int32, shape, 0)
+    column = lax.broadcasted_iota(jnp.int32, shape, 1)
+    used = row % SLAB < capacity
+    return (used & (column == row // SLAB * capacity + row % SLAB)).astype(jnp.bfloat16)
+
+
+def experts_kernel(
+    heads_ref, proj_a_ref, proj_b_ref, resid_ref, gain_ref, ids_ref, weights_ref,
+    gate_hbm, up_hbm, down_hbm, out_ref,
+    mixed, slabs, landing, returned, back, go_send, go_recv, back_send, back_recv,
+    xbuf, gate, up, down, w_sem, ag_send, ag_recv, share_send, share_recv, *exchange,
 ):
     sp, z, core = tp_place()
-    ex = Exchange(pbuf, other, stage, landed, pair_send, pair_recv, ring_send, ring_recv)
-    for first in range(0, 2048, 512):
-        cols = slice(first, first + 512)
-        term = dot32(heads_ref[:, 0:128], proj_a_ref[:, cols])
-        term = term + dot32(heads_ref[:, 128:192], proj_b_ref[:, cols])
-        pbuf[:, :, cols] = term.astype(jnp.bfloat16).reshape(16, 32, 512)
-    meet_tp(sp, z, core)
-    order = (4, 3, -3, 2, -2, 1, -1, 0)
-    for offset in order:
-        ex.pair_copy(offset).start()
-    ex.pair_copy(4).wait_recv()
-    ex.send(0, 0, 4)
-    ex.send(1, 1, 4)
-    for distance in (3, 2, 1):
-        ex.pair_copy(distance).wait_recv()
-        ex.pair_copy(-distance).wait_recv()
-        if distance == 3:
-            ex.send(0, 1, 3)
-            ex.send(1, 0, 3)
-        ex.send(0, 0, distance)
-        ex.send(1, 1, distance)
-        if distance < 3:
-            ex.send(0, 1, distance)
-            ex.send(1, 0, distance)
-    ex.pair_copy(0).wait_recv()
-    for half in range(2):
-        rows = slice(half * 16, half * 16 + 16)
-        mixed_ref[rows, :] = resid_ref[rows, :].astype(jnp.float32) + ex.last(half)
-    normed = rms_scaled(mixed_ref[...], gain_ref[...]).astype(jnp.bfloat16)
-    out_ref[...] = dot32(spread_ref[...], normed).astype(jnp.bfloat16)
-    ex.finish()
-
-
-def project(heads_out, proj_a, proj_b, resid, norm_gain, spread):
-    rows, width = resid.shape
-    vmem = pl.BlockSpec(memory_space=pltpu.VMEM)
-    return pl.pallas_call(
-        project_kernel,
-        out_shape=(
-            jax.ShapeDtypeStruct((rows, width), jnp.float32),
-            jax.ShapeDtypeStruct((spread.shape[0], width), jnp.bfloat16),
-        ),
-        in_specs=[vmem] * 6,
-        out_specs=(vmem, vmem),
-        scratch_shapes=exchange_scratch(rows, width),
-        compiler_params=pltpu.CompilerParams(collective_id=1, has_side_effects=True),
-    )(heads_out, proj_a, proj_b, resid, norm_gain[None, :], spread)
-
-
-def expert_kernel(
-    rows_ref, gate_hbm, up_hbm, down_hbm, out_ref,
-    xbuf, gate, up, down, w_sem, ag_send, ag_recv, share_send, share_recv,
-    pbuf, other, stage, landed, pair_send, pair_recv, ring_send, ring_recv,
-):
-    sp, z, core = tp_place()
-    ex = Exchange(pbuf, other, stage, landed, pair_send, pair_recv, ring_send, ring_recv)
+    px = Exchange(*exchange[:8])
+    ex = Exchange(*exchange[8:])
+    width = mixed.shape[1]
     loads = [
         pltpu.make_async_copy(src, dst, w_sem.at[i])
         for i, (src, dst) in enumerate(((gate_hbm, gate), (up_hbm, up), (down_hbm, down)))
     ]
     for load in loads:
         load.start()
-    xbuf[z * 2 + core] = rows_ref[...]
-    meet_tp(sp, z, core)
-    part = rows_ref.shape[0] // 2
+    pbuf = ex.pbuf
+    for first in range(0, width, 512):
+        cols = slice(first, first + 512)
+        term = dot32(heads_ref[:, 0:128], proj_a_ref[:, cols])
+        term = term + dot32(heads_ref[:, 128:192], proj_b_ref[:, cols])
+        px.pbuf[:, :, cols] = term.astype(jnp.bfloat16).reshape(16, 32, 512)
+    meet(sp, z, core)
+    for offset in (4, 3, -3, 2, -2, 1, -1, 0):
+        px.pair_copy(offset).start()
+    chosen = chosen_slots(ids_ref)
+    px.pair_copy(4).wait_recv()
+    px.send(0, 0, 4)
+    px.send(1, 1, 4)
+    for distance in (3, 2, 1):
+        px.pair_copy(distance).wait_recv()
+        px.pair_copy(-distance).wait_recv()
+        if distance == 3:
+            px.send(0, 1, 3)
+            px.send(1, 0, 3)
+        px.send(0, 0, distance)
+        px.send(1, 1, distance)
+        if distance < 3:
+            px.send(0, 1, distance)
+            px.send(1, 0, distance)
+    px.pair_copy(0).wait_recv()
+    for half in range(2):
+        rows = slice(half * 16, half * 16 + 16)
+        mixed[rows, :] = resid_ref[rows, :].astype(jnp.float32) + px.last(half)
+    normed = rms_scaled(mixed[...], gain_ref[...]).astype(jnp.bfloat16)
+    outgoing = dot32(chosen[0] + chosen[1], normed).astype(jnp.bfloat16)
+    slabs[...] = outgoing.reshape(16, SLAB, width)
+    for delta in range(1, 16):
+        slab_copy(slabs, landing, delta, go_send, go_recv).start()
+    landing[sp] = slabs[sp]
+    for delta in range(1, 16):
+        slab_copy(slabs, landing, delta, go_send, go_recv, arriving=True).wait_recv()
+    count = xbuf.shape[1]
+    capacity = count // 16
+    arrived = landing[...].reshape(16 * SLAB, width)
+    xbuf[z * 2 + core] = dot32(packing(count, capacity), arrived).astype(jnp.bfloat16)
+    part = count // 2
 
     def shard(offset, half):
         chip = ex.chip(offset)
@@ -423,10 +452,9 @@
         sign = 1 - 2 * way
         away = distance + 1 if arriving else distance
         offset = 4 if away == 4 else -sign * away
-        here = rows_ref.at[pl.ds(half * part, part)] if away == 0 else shard(offset, half)
         number = way * 8 + half * 4 + distance
         return pltpu.make_async_remote_copy(
-            src_ref=here,
+            src_ref=shard(offset, half),
             dst_ref=shard(offset, half),
             send_sem=ag_send.at[number],
             recv_sem=ag_recv.at[number],
@@ -437,12 +465,9 @@
     def share_copy(offset, half, arriving=False):
         chip = ex.chip(offset)
         there = xbuf.at[chip * 2 + (1 - core if arriving else core), pl.ds(half * part, part)]
-        here = there
-        if offset == 0 and not arriving:
-            here = rows_ref.at[pl.ds(half * part, part)]
         number = (offset + 3) * 2 + half
         return pltpu.make_async_remote_copy(
-            src_ref=here,
+            src_ref=there,
             dst_ref=there,
             send_sem=share_send.at[number],
             recv_sem=share_recv.at[number],
@@ -522,8 +547,31 @@
             ex.send(1, 0, distance)
         ex.send(0, 0, distance)
         ex.send(1, 1, distance)
+    widen = unpacking(part, capacity)
     for half in range(2):
-        out_ref[half * part : (half + 1) * part, :] = ex.last(half).astype(jnp.bfloat16)
+        summed = ex.last(half).astype(jnp.bfloat16)
+        spread = dot32(widen, summed).astype(jnp.bfloat16)
+        returned[half * 8 : half * 8 + 8] = spread.reshape(8, SLAB, width)
+    for delta in range(1, 16):
+        slab_copy(returned, back, delta, back_send, back_recv).start()
+    back[sp] = returned[sp]
+    tokens = mixed.shape[0]
+    row = lax.broadcasted_iota(jnp.int32, (tokens, tokens), 0)
+    same = row == lax.broadcasted_iota(jnp.int32, (tokens, tokens), 1)
+    picks = [jnp.transpose(c.astype(jnp.float32)).astype(jnp.bfloat16) for c in chosen]
+    factors = [
+        jnp.sum(jnp.where(same, weights_ref[r : r + 1, :], 0.0), axis=1, keepdims=True)
+        for r in range(2)
+    ]
+    for delta in range(1, 16):
+        slab_copy(returned, back, delta, back_send, back_recv, arriving=True).wait_recv()
+    rows = back[...].reshape(16 * SLAB, width)
+    added = factors[0] * dot32(picks[0], rows) + factors[1] * dot32(picks[1], rows)
+    out_ref[...] = (mixed[...] + added).astype(jnp.bfloat16)
+    for delta in range(1, 16):
+        slab_copy(slabs, landing, delta, go_send, go_recv).wait_send()
+        slab_copy(returned, back, delta, back_send, back_recv).wait_send()
+    px.finish()
     ex.finish()
     for way in range(2):
         for half in range(2):
@@ -534,31 +582,38 @@
             share_copy(offset, half).wait_send()
 
 
-def run_experts(rows, gate, up, down):
-    count, width = rows.shape
+def project_and_run_experts(
+    heads_out, proj_a, proj_b, resid, norm_gain, route_ids, route_weights, gate, up, down
+):
+    tokens, width = resid.shape
+    count = 3 * route_ids.shape[1] * tokens // 2
     vmem = pl.BlockSpec(memory_space=pltpu.VMEM)
     anywhere = pl.BlockSpec(memory_space=pl.ANY)
     return pl.pallas_call(
-        expert_kernel,
-        out_shape=jax.ShapeDtypeStruct((count, width), jnp.bfloat16),
-        in_specs=[vmem, anywhere, anywhere, anywhere],
+        experts_kernel,
+        out_shape=jax.ShapeDtypeStruct((tokens, width), jnp.bfloat16),
+        in_specs=[vmem] * 7 + [anywhere] * 3,
         out_specs=vmem,
-        scratch_shapes=[
+        scratch_shapes=[pltpu.VMEM((tokens, width), jnp.float32)]
+        + [pltpu.VMEM((16, SLAB, width), jnp.bfloat16)] * 4
+        + [pltpu.SemaphoreType.DMA((16,))] * 4
+        + [
             pltpu.VMEM((16, count, width), jnp.bfloat16),
             pltpu.VMEM(gate.shape, gate.dtype),
             pltpu.VMEM(up.shape, up.dtype),
             pltpu.VMEM(down.shape, down.dtype),
             pltpu.SemaphoreType.DMA((3,)),
-            pltpu.SemaphoreType.DMA((16,)),
-            pltpu.SemaphoreType.DMA((16,)),
-            pltpu.SemaphoreType.DMA((16,)),
-            pltpu.SemaphoreType.DMA((16,)),
         ]
+        + [pltpu.SemaphoreType.DMA((16,))] * 4
+        + exchange_scratch(tokens, width)
         + exchange_scratch(count, width),
         compiler_params=pltpu.CompilerParams(
-            collective_id=2, has_side_effects=True, vmem_limit_bytes=60 * 1024 * 1024
+            collective_id=1, has_side_effects=True, vmem_limit_bytes=60 * 1024 * 1024
         ),
-    )(rows, gate, up, down)
+    )(
+        heads_out, proj_a, proj_b, resid, norm_gain[None, :], route_ids.T, route_weights.T,
+        gate, up, down,
+    )
 
 
 def per_device(
@@ -582,34 +637,13 @@
     expert_up,
     expert_down,
 ):
-    sp_ways = lax.axis_size("sp")
     heads_out = attention(
         query_a, key_a, value_a, query_b, key_b, value_b, mix_a, mix_b, head_gain_a, head_gain_b
     )
-    width = resid.shape[1]
-    tok_rows = resid.shape[0]
-    top_count = route_ids.shape[1]
-    capacity = 3 * top_count * tok_rows // (2 * sp_ways)
-    own_slots = slot_numbers(route_ids, sp_ways, capacity)
-    lookup = jnp.arange(sp_ways * capacity, dtype=jnp.int32)[:, None]
-    spread = jnp.zeros((sp_ways * capacity, tok_rows), jnp.float32)
-    for which in range(top_count):
-        spread = spread + (own_slots[:, which][None, :] == lookup).astype(jnp.float32)
-    mixed, outgoing = project(
-        heads_out, proj_a, proj_b, resid, norm_gain, spread.astype(jnp.bfloat16)
-    )
-    arrived = lax.all_to_all(
-        outgoing.reshape(sp_ways, capacity, width), "sp", split_axis=0, concat_axis=0, tiled=True
-    )
-    summed = run_experts(
-        arrived.reshape(sp_ways * capacity, width), expert_gate, expert_up, expert_down
-    )
-    finished_rows = summed.reshape(sp_ways, capacity, width)
-    back = lax.all_to_all(finished_rows, "sp", split_axis=0, concat_axis=0, tiled=True)
-    picked = jnp.take(back.reshape(sp_ways * capacity, width), own_slots.reshape(-1), axis=0)
-    picked = picked.reshape(tok_rows, top_count, width)
-    output = mixed + jnp.sum(route_weights[:, :, None] * picked.astype(jnp.float32), axis=1)
-    return output.astype(jnp.bfloat16)
+    return project_and_run_experts(
+        heads_out, proj_a, proj_b, resid, norm_gain, route_ids, route_weights,
+        expert_gate, expert_up, expert_down,
+    )
 
 
 def solution(mesh):

time: 212 us -> 174 us (0.82)
  blocking collectives: 32.7 us -> 0 us
  Pallas kernels: 152 us -> 171 us
  waiting for transfers between devices: 9.55 us -> 0 us
  local copies, waits for them, and re-layouts: 6.44 us -> 1.57 us
  other arithmetic: 4.76 us -> 0 us
  starting transfers between devices: 3.57 us -> 0 us
    all_to_all x1 -> x0, blocking collectives: 32.7 us -> none  [per_device(): lax.all_to_all(outgoing.reshape(sp_ways, capacity, width), 'sp', split_ax...]
    pallas_call x2 -> x1, Pallas kernels: 102 us -> 128 us  [project_and_run_experts(): pl.pallas_call(experts_kernel, out_shape=jax.ShapeDtypeStruct((tokens, wi...]
    all_to_all x1 -> x0, waiting for transfers between devices: 9.55 us -> none  [per_device(): lax.all_to_all(finished_rows, 'sp', split_axis=0, concat_axis=0, tiled=True)]
    pallas_call x1, Pallas kernels: 50.2 us -> 42.5 us  [attention(): pl.pallas_call(attention_kernel, out_shape=jax.ShapeDtypeStruct((rows, 19...]
    reshape x4 -> x0, local copies, waits for them, and re-layouts: 4.06 us -> none  [the longest x1 1.93 us: per_device(): finished_rows = summed.reshape(sp_ways, capacity, width)]
    all_to_all x1 -> x0, starting transfers between devices: 3.57 us -> none  [per_device(): lax.all_to_all(finished_rows, 'sp', split_axis=0, concat_axis=0, tiled=True)]
  transfers between devices with their start and end apart: 1 -> 0, of which waited for: 1 -> 0; matrix products, arithmetic and copies ran while one was open for 0% -> 0% of each run, Pallas kernels for 0% -> 0%
where the time goes in v3:
time: 174 us; the launch traced here: 173 us
  Pallas kernels  171 us (98%)
    pallas_call x1, Pallas kernels, project_and_run_experts(): pl.pallas_call(experts_kernel, out_shape=jax.ShapeDtypeStruct((tokens, wi...  128 us
    pallas_call x1, Pallas kernels, attention(): pl.pallas_call(attention_kernel, out_shape=jax.ShapeDtypeStruct((rows, 19...  42.5 us

profile of v3, /device:TPU:1, one launch (start us, length us, event | category | flops | bytes accessed | tf_op | source)
XLA Modules:
  0.0 173.4 jit_solution(11979706188761477690)
XLA Ops:
  1.3 42.5 %shard_map.181.heads_ref = bf16[512,192]{1,0:T(8,128)(2,1)} custom-call(bf16[512,128]{1,0:T(8,128)(2,1)} %bitcast.17, bf16[64,512]{1,0:T(8,128)(2,1)} %bitcast.20, bf16[512,128]{1,0:T(8,128)(2,1)} %bitcast.18, bf16[512,128]{1,0:T(8,128)(2,1)} %bitcast.19, bf16[64,512]{1,0:T(8,128)(2,1)} %bitcast.21, bf16[64,512]{1,0:T(8,128)(2,1)} %bitcast.22, ...), custom_call_target="tpu_custom_call" | custom-call | tf_op jit(solution)/shard_map/pallas_call | solution.py:222
  43.8 128.1 %shard_map.182 = bf16[32,2048]{1,0:T(8,128)(2,1)} custom-call(bf16[512,192]{1,0:T(8,128)(2,1)} %shard_map.181.heads_ref, bf16[128,2048]{1,0:T(8,128)(2,1)} %proj_a_ref.1, bf16[64,2048]{1,0:T(8,128)(2,1)} %proj_b_ref.1, bf16[32,2048]{1,0:T(8,128)(2,1)} %resid_ref.1, f32[1,2048]{1,0:T(1,128)} %bitcast.23, s32[2,32]{1,0:T(2,128)} %bitcast.24, ...), custom_call_target="tpu_custom_call" | custom-call | tf_op jit(solution)/shard_map/pallas_call | solution.py:592
  171.8 1.6 copy.23

commit v4 on v3

--- a/solution.py
+++ b/solution.py
@@ -20,13 +20,14 @@
 LOG2E = 1.4426950408889634
 PART = 128
 CHUNK = 64
+PIECES = 2
 
 
 def dot32(a, b):
     return jnp.dot(a, b, preferred_element_type=jnp.float32)
 
 
-def attention_kernel(
+def attention_part(
     qa_ref, qb_ref, ka_ref, va_ref, kb_ref, vb_ref, mix_a_ref, mix_b_ref, gain_a_ref, gain_b_ref,
     out_ref,
     buf, qta, qtb, k_b, s_even, s_odd, p_even, p_odd, acc_a, acc_b, m_ref, l_ref,
@@ -44,9 +45,7 @@
     def spot(h, df, dg):
         return at(df, dg) if h == 0 else at(dg, df)
 
-    barrier = pltpu.get_barrier_semaphore()
-    for ox, oy in ((1, 0), (-1, 0), (0, 1), (0, -1)):
-        pl.semaphore_signal(barrier, inc=1, device_id=(at(ox, oy), tp), device_id_type=MESH)
+    peers = greet()
 
     va_t = jnp.transpose(va_ref[...])
     for h in range(2):
@@ -56,7 +55,7 @@
         buf[place, h, 128:192, 128:384] = kb_ref[:, cols]
         buf[place, h, 192:256, 128:384] = vb_ref[:, cols]
 
-    pl.semaphore_wait(barrier, 4)
+    pl.semaphore_wait(pltpu.get_barrier_semaphore(), peers)
 
     def region(h, df, dg, part):
         ref = buf.at[spot(h, df, dg), h]
@@ -167,8 +166,9 @@
 
     plan = (
         ((-1, 0), ()), ((0, -1), (4, 5)), ((1, 0), ()), ((0, 1), (6, 7)), ((-1, -1), ()),
-        ((1, -1), (8, 9)), ((-1, 1), ()), ((1, 1), ()), ((2, 0), (10, 11, 12, 13)), ((0, 2), ()),
-        ((2, -1), (14, 15)), ((-1, 2), ()), ((2, 1), (16, 17)), ((1, 2), ()), ((2, 2), (18, 19)),
+        ((2, 0), (12, 13)), ((0, 2), (8, 9)), ((1, -1), ()), ((-1, 1), ()), ((1, 1), ()),
+        ((2, -1), (10, 11, 14, 15)), ((-1, 2), (16, 17)), ((2, 1), ()), ((1, 2), (18, 19)),
+        ((2, 2), ()),
     )
     follow = {5: (10, 11), 6: (14,), 7: (15,), 8: (16,), 9: (17,), 10: (18,), 11: (19,)}
 
@@ -194,9 +194,9 @@
 
     block(place, (0, half))
     arrive(0, 4, 6, 7)
-    arrive(1, 5, 8, 9)
+    arrive(1, 5)
     arrive(2, 12)
-    arrive(3, 13)
+    arrive(3, 13, 8, 9)
     lax.fori_loop(0, len(plan), step, 0)
 
     for h in range(2):
@@ -211,41 +211,13 @@
             out_ref[h * half : (h + 1) * half, first : first + rows.shape[1]] = rows.astype(
                 jnp.bfloat16
             )
-    for number in range(20):
-        for h in range(2):
-            copy(h, number, *moves[number]).wait_send()
-
-
-def attention(query_a, key_a, value_a, query_b, key_b, value_b, mix_a, mix_b, gain_a, gain_b):
-    rows = query_a.shape[0]
-    vmem = pl.BlockSpec(memory_space=pltpu.VMEM)
-    return pl.pallas_call(
-        attention_kernel,
-        out_shape=jax.ShapeDtypeStruct((rows, 192), jnp.bfloat16),
-        in_specs=[vmem] * 6 + [pl.BlockSpec(memory_space=pltpu.SMEM)] * 2 + [vmem] * 2,
-        out_specs=vmem,
-        scratch_shapes=[
-            pltpu.VMEM((16, 2, 256, 384), jnp.bfloat16),
-            pltpu.VMEM((4, 128, 256), jnp.bfloat16),
-            pltpu.VMEM((4, 64, 256), jnp.bfloat16),
-            pltpu.VMEM((2, 256, 64), jnp.bfloat16),
-            pltpu.VMEM((512, 256), jnp.float32),
-            pltpu.VMEM((512, 256), jnp.float32),
-            pltpu.VMEM((512, 256), jnp.bfloat16),
-            pltpu.VMEM((512, 256), jnp.bfloat16),
-            pltpu.VMEM((4, 128, 256), jnp.float32),
-            pltpu.VMEM((4, 64, 256), jnp.float32),
-            pltpu.VMEM((8, 1, 256), jnp.float32),
-            pltpu.VMEM((8, 8, 256), jnp.float32),
-            pltpu.SemaphoreType.DMA((40,)),
-            pltpu.SemaphoreType.DMA((40,)),
-        ],
-        compiler_params=pltpu.CompilerParams(collective_id=0, has_side_effects=True),
-    )(
-        query_a[:, 0, :], query_b[:, 0, :].T, key_a[:, 0, :], value_a[:, 0, :],
-        key_b[:, 0, :].T, value_b[:, 0, :].T,
-        mix_a, mix_b, gain_a[None, :], gain_b[None, :],
-    )
+
+    def finish():
+        for number in range(20):
+            for h in range(2):
+                copy(h, number, *moves[number]).wait_send()
+
+    return finish
 
 
 def tp_place():
@@ -253,14 +225,15 @@
     return lax.axis_index("sp"), tp // 2, tp % 2
 
 
-def meet(sp, z, core):
+def greet():
+    sp, z, core = tp_place()
     tp = z * 2 + core
     barrier = pltpu.get_barrier_semaphore()
     peers = [(sp, ((z + 1) % 8) * 2 + core), (sp, ((z + 7) % 8) * 2 + core), (sp, tp + 1 - 2 * core)]
     peers += [((sp + delta) % 16, tp) for delta in range(1, 16)]
     for peer in peers:
         pl.semaphore_signal(barrier, inc=1, device_id=peer, device_id_type=MESH)
-    pl.semaphore_wait(barrier, len(peers))
+    return len(peers)
 
 
 class Exchange:
@@ -268,7 +241,7 @@
         self.sp, self.z, self.core = tp_place()
         self.pbuf, self.other, self.stage, self.landed = pbuf, other, stage, landed
         self.pair_sems, self.ring_sems = (pair_send, pair_recv), (ring_send, ring_recv)
-        self.rows = pbuf.shape[1] // 2
+        self.rows, self.wide = pbuf.shape[1] // 2, pbuf.shape[2] // PIECES
 
     def chip(self, offset):
         return (self.z + offset + 8) % 8
@@ -284,36 +257,40 @@
             device_id_type=MESH,
         )
 
-    def ring_copy(self, way, half, distance):
-        number = way * 8 + half * 4 + distance - 1
+    def ring_copy(self, way, half, distance, piece):
+        number = ((way * 2 + half) * 4 + distance - 1) * PIECES + piece
+        columns = pl.ds(piece * self.wide, self.wide)
         return pltpu.make_async_remote_copy(
-            src_ref=self.stage.at[way, half, distance - 1],
-            dst_ref=self.landed.at[way, half, distance - 1],
+            src_ref=self.stage.at[way, half, distance - 1, :, columns],
+            dst_ref=self.landed.at[way, half, distance - 1, :, columns],
             send_sem=self.ring_sems[0].at[number],
             recv_sem=self.ring_sems[1].at[number],
             device_id=(self.sp, self.chip(1 - 2 * way) * 2 + self.core),
             device_id_type=MESH,
         )
 
-    def mine(self, offset, half):
+    def mine(self, offset, half, columns=slice(None)):
         chip = self.chip(offset)
         rows = slice(half * self.rows, (half + 1) * self.rows)
-        own = self.pbuf[chip * 2 + self.core, rows, :].astype(jnp.float32)
-        return own + self.other[chip, rows, :].astype(jnp.float32)
+        own = self.pbuf[chip * 2 + self.core, rows, columns].astype(jnp.float32)
+        return own + self.other[chip, rows, columns].astype(jnp.float32)
 
     def send(self, way, half, distance):
         offset = distance * (1 - 2 * way)
-        total = self.mine(4 if distance == 4 else offset, half)
-        if distance < (4 if half == way else 3):
-            self.ring_copy(way, half, distance + 1).wait_recv()
-            total = total + self.landed[way, half, distance].astype(jnp.float32)
-        self.stage[way, half, distance - 1] = total.astype(jnp.bfloat16)
-        self.ring_copy(way, half, distance).start()
+        for piece in range(PIECES):
+            columns = slice(piece * self.wide, (piece + 1) * self.wide)
+            total = self.mine(4 if distance == 4 else offset, half, columns)
+            if distance < (4 if half == way else 3):
+                self.ring_copy(way, half, distance + 1, piece).wait_recv()
+                total = total + self.landed[way, half, distance, :, columns].astype(jnp.float32)
+            self.stage[way, half, distance - 1, :, columns] = total.astype(jnp.bfloat16)
+            self.ring_copy(way, half, distance, piece).start()
 
     def last(self, half):
         total = self.mine(0, half)
         for way in range(2):
-            self.ring_copy(way, half, 1).wait_recv()
+            for piece in range(PIECES):
+                self.ring_copy(way, half, 1, piece).wait_recv()
             total = total + self.landed[way, half, 0].astype(jnp.float32)
         return total
 
@@ -323,7 +300,8 @@
         for way in range(2):
             for half in range(2):
                 for distance in range(1, 5 if half == way else 4):
-                    self.ring_copy(way, half, distance).wait_send()
+                    for piece in range(PIECES):
+                        self.ring_copy(way, half, distance, piece).wait_send()
 
 
 def exchange_scratch(rows, width):
@@ -334,8 +312,8 @@
         pltpu.VMEM((2, 2, 4, rows // 2, width), jnp.bfloat16),
         pltpu.SemaphoreType.DMA((8,)),
         pltpu.SemaphoreType.DMA((8,)),
-        pltpu.SemaphoreType.DMA((16,)),
-        pltpu.SemaphoreType.DMA((16,)),
+        pltpu.SemaphoreType.DMA((16 * PIECES,)),
+        pltpu.SemaphoreType.DMA((16 * PIECES,)),
     ]
 
 
@@ -386,7 +364,7 @@
     return (used & (column == row // SLAB * capacity + row % SLAB)).astype(jnp.bfloat16)
 
 
-def experts_kernel(
+def experts_part(
     heads_ref, proj_a_ref, proj_b_ref, resid_ref, gain_ref, ids_ref, weights_ref,
     gate_hbm, up_hbm, down_hbm, out_ref,
     mixed, slabs, landing, returned, back, go_send, go_recv, back_send, back_recv,
@@ -396,19 +374,12 @@
     px = Exchange(*exchange[:8])
     ex = Exchange(*exchange[8:])
     width = mixed.shape[1]
-    loads = [
-        pltpu.make_async_copy(src, dst, w_sem.at[i])
-        for i, (src, dst) in enumerate(((gate_hbm, gate), (up_hbm, up), (down_hbm, down)))
-    ]
-    for load in loads:
-        load.start()
     pbuf = ex.pbuf
     for first in range(0, width, 512):
         cols = slice(first, first + 512)
         term = dot32(heads_ref[:, 0:128], proj_a_ref[:, cols])
         term = term + dot32(heads_ref[:, 128:192], proj_b_ref[:, cols])
         px.pbuf[:, :, cols] = term.astype(jnp.bfloat16).reshape(16, 32, 512)
-    meet(sp, z, core)
     for offset in (4, 3, -3, 2, -2, 1, -1, 0):
         px.pair_copy(offset).start()
     chosen = chosen_slots(ids_ref)
@@ -512,7 +483,7 @@
         came(0, 1, distance)
         came(1, 0, distance)
         if distance == 1:
-            for load in loads:
+            for load in weight_loads(gate_hbm, up_hbm, down_hbm, gate, up, down, w_sem):
                 load.wait()
             feed(0)
             experts(0, 1)
@@ -582,38 +553,22 @@
             share_copy(offset, half).wait_send()
 
 
-def project_and_run_experts(
-    heads_out, proj_a, proj_b, resid, norm_gain, route_ids, route_weights, gate, up, down
-):
-    tokens, width = resid.shape
-    count = 3 * route_ids.shape[1] * tokens // 2
-    vmem = pl.BlockSpec(memory_space=pltpu.VMEM)
-    anywhere = pl.BlockSpec(memory_space=pl.ANY)
-    return pl.pallas_call(
-        experts_kernel,
-        out_shape=jax.ShapeDtypeStruct((tokens, width), jnp.bfloat16),
-        in_specs=[vmem] * 7 + [anywhere] * 3,
-        out_specs=vmem,
-        scratch_shapes=[pltpu.VMEM((tokens, width), jnp.float32)]
-        + [pltpu.VMEM((16, SLAB, width), jnp.bfloat16)] * 4
-        + [pltpu.SemaphoreType.DMA((16,))] * 4
-        + [
-            pltpu.VMEM((16, count, width), jnp.bfloat16),
-            pltpu.VMEM(gate.shape, gate.dtype),
-            pltpu.VMEM(up.shape, up.dtype),
-            pltpu.VMEM(down.shape, down.dtype),
-            pltpu.SemaphoreType.DMA((3,)),
-        ]
-        + [pltpu.SemaphoreType.DMA((16,))] * 4
-        + exchange_scratch(tokens, width)
-        + exchange_scratch(count, width),
-        compiler_params=pltpu.CompilerParams(
-            collective_id=1, has_side_effects=True, vmem_limit_bytes=60 * 1024 * 1024
-        ),
-    )(
-        heads_out, proj_a, proj_b, resid, norm_gain[None, :], route_ids.T, route_weights.T,
-        gate, up, down,
-    )
+def weight_loads(gate_hbm, up_hbm, down_hbm, gate, up, down, w_sem):
+    pairs = ((gate_hbm, gate), (up_hbm, up), (down_hbm, down))
+    return [pltpu.make_async_copy(a, b, w_sem.at[i]) for i, (a, b) in enumerate(pairs)]
+
+
+ATTENTION_INPUTS, ATTENTION_SCRATCH = 10, 14
+
+
+def whole_kernel(*refs):
+    inputs, (out_ref, heads), scratch = refs[:19], refs[19:21], refs[21:]
+    own, rest = scratch[:ATTENTION_SCRATCH], scratch[ATTENTION_SCRATCH:]
+    for load in weight_loads(*inputs[16:19], *rest[10:14]):
+        load.start()
+    finish = attention_part(*inputs[:ATTENTION_INPUTS], heads, *own)
+    experts_part(heads, *inputs[ATTENTION_INPUTS:], out_ref, *rest)
+    finish()
 
 
 def per_device(
@@ -637,11 +592,56 @@
     expert_up,
     expert_down,
 ):
-    heads_out = attention(
-        query_a, key_a, value_a, query_b, key_b, value_b, mix_a, mix_b, head_gain_a, head_gain_b
-    )
-    return project_and_run_experts(
-        heads_out, proj_a, proj_b, resid, norm_gain, route_ids, route_weights,
+    tokens, width = resid.shape
+    rows = query_a.shape[0]
+    half = rows // 2
+    count = 3 * route_ids.shape[1] * tokens // 2
+    vmem = pl.BlockSpec(memory_space=pltpu.VMEM)
+    smem = pl.BlockSpec(memory_space=pltpu.SMEM)
+    anywhere = pl.BlockSpec(memory_space=pl.ANY)
+    attention_scratch = [
+        pltpu.VMEM((16, 2, half, 384), jnp.bfloat16),
+        pltpu.VMEM((4, 128, half), jnp.bfloat16),
+        pltpu.VMEM((4, 64, half), jnp.bfloat16),
+        pltpu.VMEM((2, half, 64), jnp.bfloat16),
+        pltpu.VMEM((rows, half), jnp.float32),
+        pltpu.VMEM((rows, half), jnp.float32),
+        pltpu.VMEM((rows, half), jnp.bfloat16),
+        pltpu.VMEM((rows, half), jnp.bfloat16),
+        pltpu.VMEM((4, 128, half), jnp.float32),
+        pltpu.VMEM((4, 64, half), jnp.float32),
+        pltpu.VMEM((8, 1, half), jnp.float32),
+        pltpu.VMEM((8, 8, half), jnp.float32),
+        pltpu.SemaphoreType.DMA((40,)),
+        pltpu.SemaphoreType.DMA((40,)),
+    ]
+    experts_scratch = [
+        pltpu.VMEM((tokens, width), jnp.float32),
+        *[pltpu.VMEM((16, SLAB, width), jnp.bfloat16)] * 4,
+        *[pltpu.SemaphoreType.DMA((16,))] * 4,
+        pltpu.VMEM((16, count, width), jnp.bfloat16),
+        pltpu.VMEM(expert_gate.shape, expert_gate.dtype),
+        pltpu.VMEM(expert_up.shape, expert_up.dtype),
+        pltpu.VMEM(expert_down.shape, expert_down.dtype),
+        pltpu.SemaphoreType.DMA((3,)),
+        *[pltpu.SemaphoreType.DMA((16,))] * 4,
+        *exchange_scratch(tokens, width),
+        *exchange_scratch(count, width),
+    ]
+    return pl.pallas_call(
+        whole_kernel,
+        out_shape=jax.ShapeDtypeStruct((tokens, width), jnp.bfloat16),
+        in_specs=[vmem] * 6 + [smem] * 2 + [vmem] * 8 + [anywhere] * 3,
+        out_specs=vmem,
+        scratch_shapes=[pltpu.VMEM((rows, 192), jnp.bfloat16), *attention_scratch, *experts_scratch],
+        compiler_params=pltpu.CompilerParams(
+            collective_id=0, has_side_effects=True, vmem_limit_bytes=60 * 1024 * 1024
+        ),
+    )(
+        query_a[:, 0, :], query_b[:, 0, :].T, key_a[:, 0, :], value_a[:, 0, :],
+        key_b[:, 0, :].T, value_b[:, 0, :].T,
+        mix_a, mix_b, head_gain_a[None, :], head_gain_b[None, :],
+        proj_a, proj_b, resid, norm_gain[None, :], route_ids.T, route_weights.T,
         expert_gate, expert_up, expert_down,
     )
 

time: 174 us -> 166 us (0.954)
  Pallas kernels: 171 us -> 163 us
    pallas_call x2 -> x1, Pallas kernels: 171 us -> 163 us  [per_device(): pl.pallas_call(whole_kernel, out_shape=jax.ShapeDtypeStruct((tokens, widt...]
where the time goes in v4:
time: 166 us; the launch traced here: 165 us
  Pallas kernels  163 us (98%)
    pallas_call x1, Pallas kernels, per_device(): pl.pallas_call(whole_kernel, out_shape=jax.ShapeDtypeStruct((tokens, widt...  163 us

profile of v4, /device:TPU:1, one launch (start us, length us, event | category | flops | bytes accessed | tf_op | source)
XLA Modules:
  0.0 165.4 jit_solution(13434763572378383811)
XLA Ops:
  1.3 162.6 %shard_map.181 = bf16[32,2048]{1,0:T(8,128)(2,1)} custom-call(bf16[512,128]{1,0:T(8,128)(2,1)} %bitcast.17, bf16[64,512]{1,0:T(8,128)(2,1)} %bitcast.20, bf16[512,128]{1,0:T(8,128)(2,1)} %bitcast.18, bf16[512,128]{1,0:T(8,128)(2,1)} %bitcast.19, bf16[64,512]{1,0:T(8,128)(2,1)} %bitcast.21, bf16[64,512]{1,0:T(8,128)(2,1)} %bitcast.22, f32[1]{0:T(128)S(6)} %copy.21.refs_6_, ...), custom_call_target="tpu_custom_call" | custom-call | tf_op jit(solution)/shard_map/pallas_call | solution.py:631
  163.9 1.6 copy.23

commit v5 on v4

--- a/solution.py
+++ b/solution.py
@@ -20,7 +20,7 @@
 LOG2E = 1.4426950408889634
 PART = 128
 CHUNK = 64
-PIECES = 2
+PIECES = 4
 
 
 def dot32(a, b):
@@ -30,10 +30,10 @@
 def attention_part(
     qa_ref, qb_ref, ka_ref, va_ref, kb_ref, vb_ref, mix_a_ref, mix_b_ref, gain_a_ref, gain_b_ref,
     out_ref,
-    buf, qta, qtb, k_b, s_even, s_odd, p_even, p_odd, acc_a, acc_b, m_ref, l_ref,
+    buf, qta, qtb, k_b, s_0, s_1, s_2, s_3, p_0, p_1, p_2, p_3, acc_a, acc_b, m_ref, l_ref,
     send_sem, recv_sem,
 ):
-    s_refs, p_refs = (s_even, s_odd), (p_even, p_odd)
+    s_refs, p_refs = (s_0, s_1, s_2, s_3), (p_0, p_1, p_2, p_3)
     place = lax.axis_index("sp")
     tp = lax.axis_index("tp")
     y, x = place // 4, place % 4
@@ -127,7 +127,7 @@
                 query_pos = (index % 2) * half + lax.broadcasted_iota(jnp.int32, (half, half), 1)
                 key_pos = offsets[h] + lax.broadcasted_iota(jnp.int32, (half, half), 0)
                 found = jnp.where(key_pos <= query_pos, found, NEG)
-            s_refs[place_in][h * half : (h + 1) * half, :] = found
+            s_refs[number % 4][h * half : (h + 1) * half, :] = found
             most = jnp.max(found.reshape(half // 8, 8, half), axis=0)
             top = most if top is None else jnp.maximum(top, most)
         return jnp.max(top, axis=0, keepdims=True)
@@ -142,27 +142,27 @@
         sums = l_ref[slot] * scale
         for first in range(0, 2 * half, CHUNK):
             rows = slice(first, first + CHUNK)
-            weights = jnp.exp2((s_refs[group][rows, :] - fresh) * factor)
+            weights = jnp.exp2((s_refs[number % 4][rows, :] - fresh) * factor)
             sums = sums + jnp.sum(weights.reshape(CHUNK // 8, 8, half), axis=0)
-            p_refs[group][rows, :] = weights.astype(jnp.bfloat16)
+            p_refs[number % 4][rows, :] = weights.astype(jnp.bfloat16)
         l_ref[slot] = sums
         return scale
 
     def gather(number, source, scale):
         index, group = number // 2, number % 2
         acc, rows = (acc_b, slice(192, 256)) if group else (acc_a, slice(0, 128))
-        added = dot32(buf[source, 0, rows, 128:384], p_refs[group][0:half, :])
-        added = added + dot32(buf[source, 1, rows, 128:384], p_refs[group][half : 2 * half, :])
+        added = dot32(buf[source, 0, rows, 128:384], p_refs[number % 4][0:half, :])
+        added = added + dot32(buf[source, 1, rows, 128:384], p_refs[number % 4][half : 2 * half, :])
         acc[index] = acc[index] * scale + added
 
     def block(source, offsets):
         for h in range(2):
             k_b[h] = jnp.transpose(buf[source, h, 128:192, 128:384])
-        top = score(0, source, offsets)
+        tops = [score(number, source, offsets) for number in range(2)]
         for number in range(8):
-            later = score(number + 1, source, offsets) if number < 7 else None
-            gather(number, source, soften(number, top))
-            top = later
+            if number + 2 < 8:
+                tops.append(score(number + 2, source, offsets))
+            gather(number, source, soften(number, tops[number]))
 
     plan = (
         ((-1, 0), ()), ((0, -1), (4, 5)), ((1, 0), ()), ((0, 1), (6, 7)), ((-1, -1), ()),
@@ -246,16 +246,28 @@
     def chip(self, offset):
         return (self.z + offset + 8) % 8
 
-    def pair_copy(self, offset):
+    def pair_copy(self, offset, half):
         chip = self.chip(offset)
+        rows = pl.ds(half * self.rows, self.rows)
+        number = (offset + 3) * 2 + half
         return pltpu.make_async_remote_copy(
-            src_ref=self.pbuf.at[chip * 2 + 1 - self.core],
-            dst_ref=self.other.at[chip],
-            send_sem=self.pair_sems[0].at[offset + 3],
-            recv_sem=self.pair_sems[1].at[offset + 3],
+            src_ref=self.pbuf.at[chip * 2 + 1 - self.core, rows],
+            dst_ref=self.other.at[chip, rows],
+            send_sem=self.pair_sems[0].at[number],
+            recv_sem=self.pair_sems[1].at[number],
             device_id=(self.sp, self.z * 2 + 1 - self.core),
             device_id_type=MESH,
         )
+
+    def give(self, *offsets):
+        for offset in offsets:
+            for half in range(2):
+                self.pair_copy(offset, half).start()
+
+    def take(self, *offsets):
+        for offset in offsets:
+            for half in range(2):
+                self.pair_copy(offset, half).wait_recv()
 
     def ring_copy(self, way, half, distance, piece):
         number = ((way * 2 + half) * 4 + distance - 1) * PIECES + piece
@@ -296,7 +308,8 @@
 
     def finish(self):
         for offset in range(-3, 5):
-            self.pair_copy(offset).wait_send()
+            for half in range(2):
+                self.pair_copy(offset, half).wait_send()
         for way in range(2):
             for half in range(2):
                 for distance in range(1, 5 if half == way else 4):
@@ -310,8 +323,8 @@
         pltpu.VMEM((8, rows, width), jnp.bfloat16),
         pltpu.VMEM((2, 2, 4, rows // 2, width), jnp.bfloat16),
         pltpu.VMEM((2, 2, 4, rows // 2, width), jnp.bfloat16),
-        pltpu.SemaphoreType.DMA((8,)),
-        pltpu.SemaphoreType.DMA((8,)),
+        pltpu.SemaphoreType.DMA((16,)),
+        pltpu.SemaphoreType.DMA((16,)),
         pltpu.SemaphoreType.DMA((16 * PIECES,)),
         pltpu.SemaphoreType.DMA((16 * PIECES,)),
     ]
@@ -380,15 +393,13 @@
         term = dot32(heads_ref[:, 0:128], proj_a_ref[:, cols])
         term = term + dot32(heads_ref[:, 128:192], proj_b_ref[:, cols])
         px.pbuf[:, :, cols] = term.astype(jnp.bfloat16).reshape(16, 32, 512)
-    for offset in (4, 3, -3, 2, -2, 1, -1, 0):
-        px.pair_copy(offset).start()
+    px.give(4, 3, -3, 2, -2, 1, -1, 0)
     chosen = chosen_slots(ids_ref)
-    px.pair_copy(4).wait_recv()
+    px.take(4)
     px.send(0, 0, 4)
     px.send(1, 1, 4)
     for distance in (3, 2, 1):
-        px.pair_copy(distance).wait_recv()
-        px.pair_copy(-distance).wait_recv()
+        px.take(distance, -distance)
         if distance == 3:
             px.send(0, 1, 3)
             px.send(1, 0, 3)
@@ -397,7 +408,7 @@
         if distance < 3:
             px.send(0, 1, distance)
             px.send(1, 0, distance)
-    px.pair_copy(0).wait_recv()
+    px.take(0)
     for half in range(2):
         rows = slice(half * 16, half * 16 + 16)
         mixed[rows, :] = resid_ref[rows, :].astype(jnp.float32) + px.last(half)
@@ -457,61 +468,82 @@
         for half in range(2):
             share_copy(offset, half, arriving=True).wait_recv()
 
+    def feed_half(offset, half):
+        share_copy(offset, half, arriving=True).wait_recv()
+
+    def run(chip, rows, count):
+        piece = xbuf[pl.ds(chip * 2, 2), rows].reshape(2 * count, width)
+        gated = dot32(piece, gate[0])
+        upward = dot32(piece, up[0])
+        hidden = (jax.nn.silu(gated) * upward).astype(jnp.bfloat16)
+        for begin in range(0, width, 512):
+            cols = slice(begin, begin + 512)
+            term = dot32(hidden, down[0, :, cols]).astype(jnp.bfloat16)
+            pbuf[pl.ds(chip * 2, 2), rows, cols] = term.reshape(2, count, 512)
+
     def experts(first, count):
         def step(number, carry):
+            run(ex.chip(first - 2 * first * number), pl.ds(0, 2 * part), 2 * part)
+            return carry
+
+        lax.fori_loop(0, count, step, 0)
+
+    def experts_halves(first):
+        def step(number, carry):
             chip = ex.chip(first - 2 * first * number)
-            piece = xbuf[pl.ds(chip * 2, 2)].reshape(4 * part, xbuf.shape[2])
-            gated = dot32(piece, gate[0])
-            upward = dot32(piece, up[0])
-            hidden = (jax.nn.silu(gated) * upward).astype(jnp.bfloat16)
-            for begin in range(0, xbuf.shape[2], 512):
-                cols = slice(begin, begin + 512)
-                term = dot32(hidden, down[0, :, cols]).astype(jnp.bfloat16)
-                pbuf[pl.ds(chip * 2, 2), :, cols] = term.reshape(2, 2 * part, 512)
+            run(chip, pl.ds(pl.multiple_of(number * part, part), part), part)
             return carry
 
-        lax.fori_loop(0, count, step, 0)
+        lax.fori_loop(0, 2, step, 0)
 
     for way in range(2):
         ag_copy(way, way, 0).start()
         ag_copy(way, 1 - way, 0).start()
     for half in range(2):
         share_copy(0, half).start()
-    for distance in (1, 2, 3):
+    for load in weight_loads(gate_hbm, up_hbm, down_hbm, gate, up, down, w_sem):
+        load.wait()
+    feed(0)
+    experts(0, 1)
+    ex.give(0)
+    for distance in (1, 2):
         came(0, 0, distance)
         came(1, 1, distance)
         came(0, 1, distance)
         came(1, 0, distance)
-        if distance == 1:
-            for load in weight_loads(gate_hbm, up_hbm, down_hbm, gate, up, down, w_sem):
-                load.wait()
-            feed(0)
-            experts(0, 1)
-            ex.pair_copy(0).start()
-        else:
-            feed(1 - distance)
-            feed(distance - 1)
-            experts(distance - 1, 2)
-            ex.pair_copy(1 - distance).start()
-            ex.pair_copy(distance - 1).start()
-    feed(-3)
-    feed(3)
-    experts(3, 2)
-    ex.pair_copy(-3).start()
-    ex.pair_copy(3).start()
+        feed(-distance)
+        feed(distance)
+        experts(distance, 2)
+        ex.give(-distance, distance)
+    came(0, 0, 3)
+    came(1, 1, 3)
+    feed_half(-3, 0)
+    feed_half(3, 1)
+    experts_halves(-3)
+    ex.pair_copy(-3, 0).start()
+    ex.pair_copy(3, 1).start()
+    came(0, 1, 3)
+    came(1, 0, 3)
+    ex.pair_copy(3, 1).wait_recv()
+    ex.send(0, 1, 3)
+    ex.pair_copy(-3, 0).wait_recv()
+    ex.send(1, 0, 3)
+    feed_half(3, 0)
+    feed_half(-3, 1)
+    experts_halves(3)
+    ex.pair_copy(3, 0).start()
+    ex.pair_copy(-3, 1).start()
     came(0, 0, 4)
     came(1, 1, 4)
-    ex.pair_copy(3).wait_recv()
-    ex.send(0, 1, 3)
-    ex.pair_copy(-3).wait_recv()
-    ex.send(1, 0, 3)
     feed(4)
     experts(4, 1)
-    ex.pair_copy(4).start()
-    for offset in (2, -2, 1, -1, 0, 4):
-        ex.pair_copy(offset).wait_recv()
+    ex.give(4)
+    ex.take(4)
     ex.send(0, 0, 4)
     ex.send(1, 1, 4)
+    ex.pair_copy(3, 0).wait_recv()
+    ex.pair_copy(-3, 1).wait_recv()
+    ex.take(2, -2, 1, -1, 0)
     for distance in (3, 2, 1):
         if distance < 3:
             ex.send(0, 1, distance)
@@ -558,7 +590,7 @@
     return [pltpu.make_async_copy(a, b, w_sem.at[i]) for i, (a, b) in enumerate(pairs)]
 
 
-ATTENTION_INPUTS, ATTENTION_SCRATCH = 10, 14
+ATTENTION_INPUTS, ATTENTION_SCRATCH = 10, 18
 
 
 def whole_kernel(*refs):
@@ -604,10 +636,8 @@
         pltpu.VMEM((4, 128, half), jnp.bfloat16),
         pltpu.VMEM((4, 64, half), jnp.bfloat16),
         pltpu.VMEM((2, half, 64), jnp.bfloat16),
-        pltpu.VMEM((rows, half), jnp.float32),
-        pltpu.VMEM((rows, half), jnp.float32),
-        pltpu.VMEM((rows, half), jnp.bfloat16),
-        pltpu.VMEM((rows, half), jnp.bfloat16),
+        *[pltpu.VMEM((rows, half), jnp.float32)] * 4,
+        *[pltpu.VMEM((rows, half), jnp.bfloat16)] * 4,
         pltpu.VMEM((4, 128, half), jnp.float32),
         pltpu.VMEM((4, 64, half), jnp.float32),
         pltpu.VMEM((8, 1, half), jnp.float32),

time: 166 us -> 161 us (0.970)
  Pallas kernels: 163 us -> 158 us
    pallas_call x1, Pallas kernels: 163 us -> 158 us  [per_device(): pl.pallas_call(whole_kernel, out_shape=jax.ShapeDtypeStruct((tokens, widt...]
where the time goes in v5:
time: 161 us
  Pallas kernels  158 us (98%)
    pallas_call x1, Pallas kernels, per_device(): pl.pallas_call(whole_kernel, out_shape=jax.ShapeDtypeStruct((tokens, widt...  158 us

profile of v5, /device:TPU:1, one launch (start us, length us, event | category | flops | bytes accessed | tf_op | source)
XLA Modules:
  0.0 160.8 jit_solution(9038591165357944573)
XLA Ops:
  1.3 157.9 %shard_map.181 = bf16[32,2048]{1,0:T(8,128)(2,1)} custom-call(bf16[512,128]{1,0:T(8,128)(2,1)} %bitcast.17, bf16[64,512]{1,0:T(8,128)(2,1)} %bitcast.20, bf16[512,128]{1,0:T(8,128)(2,1)} %bitcast.18, bf16[512,128]{1,0:T(8,128)(2,1)} %bitcast.19, bf16[64,512]{1,0:T(8,128)(2,1)} %bitcast.21, bf16[64,512]{1,0:T(8,128)(2,1)} %bitcast.22, f32[1]{0:T(128)S(6)} %copy.21.refs_6_, ...), custom_call_target="tpu_custom_call" | custom-call | tf_op jit(solution)/shard_map/pallas_call | solution.py:661
  159.2 1.6 copy.23

commit v6 on v5

--- a/solution.py
+++ b/solution.py
@@ -19,7 +19,7 @@
 MESH = pl.DeviceIdType.MESH
 LOG2E = 1.4426950408889634
 PART = 128
-CHUNK = 64
+CHUNK = 32
 PIECES = 4
 
 
@@ -570,7 +570,7 @@
         slab_copy(returned, back, delta, back_send, back_recv, arriving=True).wait_recv()
     rows = back[...].reshape(16 * SLAB, width)
     added = factors[0] * dot32(picks[0], rows) + factors[1] * dot32(picks[1], rows)
-    out_ref[...] = (mixed[...] + added).astype(jnp.bfloat16)
+    out_ref[...] = mixed[...] + added
     for delta in range(1, 16):
         slab_copy(slabs, landing, delta, go_send, go_recv).wait_send()
         slab_copy(returned, back, delta, back_send, back_recv).wait_send()
@@ -658,9 +658,9 @@
         *exchange_scratch(tokens, width),
         *exchange_scratch(count, width),
     ]
-    return pl.pallas_call(
+    output = pl.pallas_call(
         whole_kernel,
-        out_shape=jax.ShapeDtypeStruct((tokens, width), jnp.bfloat16),
+        out_shape=jax.ShapeDtypeStruct((tokens, width), jnp.float32),
         in_specs=[vmem] * 6 + [smem] * 2 + [vmem] * 8 + [anywhere] * 3,
         out_specs=vmem,
         scratch_shapes=[pltpu.VMEM((rows, 192), jnp.bfloat16), *attention_scratch, *experts_scratch],
@@ -674,6 +674,7 @@
         proj_a, proj_b, resid, norm_gain[None, :], route_ids.T, route_weights.T,
         expert_gate, expert_up, expert_down,
     )
+    return output.astype(jnp.bfloat16)
 
 
 def solution(mesh):

time: 161 us -> 160 us (level)
  other arithmetic: 0 us -> 1.62 us
    convert_element_type x0 -> x1, other arithmetic: none -> 1.62 us  [per_device(): return output.astype(jnp.bfloat16)]
where the time goes in v6:
time: 160 us
  Pallas kernels  157 us (98%)
  other arithmetic  1.62 us (1%)
    pallas_call x1, Pallas kernels, per_device(): pl.pallas_call(whole_kernel, out_shape=jax.ShapeDtypeStruct((tokens, widt...  157 us

profile of v6, /device:TPU:1, one launch (start us, length us, event | category | flops | bytes accessed | tf_op | source)
XLA Modules:
  0.0 160.2 jit_solution(2180333768888205364)
XLA Ops:
  1.3 157.2 %shard_map.181 = f32[32,2048]{1,0:T(8,128)} custom-call(bf16[512,128]{1,0:T(8,128)(2,1)} %bitcast.17, bf16[64,512]{1,0:T(8,128)(2,1)} %bitcast.20, bf16[512,128]{1,0:T(8,128)(2,1)} %bitcast.18, bf16[512,128]{1,0:T(8,128)(2,1)} %bitcast.19, bf16[64,512]{1,0:T(8,128)(2,1)} %bitcast.21, bf16[64,512]{1,0:T(8,128)(2,1)} %bitcast.22, f32[1]{0:T(128)S(6)} %copy.20.refs_6_, ...), custom_call_target="tpu_custom_call" | custom-call | tf_op jit(solution)/shard_map/pallas_call | solution.py:661
  158.5 1.6 %convert_element_type.3 = bf16[32,2048]{1,0:T(8,128)(2,1)} convert(f32[32,2048]{1,0:T(8,128)} %shard_map.181) | non-fusion elementwise | flops 65536 | bytes 393216 | tf_op jit(solution)/shard_map/convert_element_type | solution.py:677
